TPU v7x, 512 devices: a whole 4x4x16 slice. The times are simulated.
512 devices in a mesh: ep: 32 (over z, core), tp: 16 (over y, x).
Axes of the slice: x: 4, y: 4, z: 16, core: 2. Of those that a mesh axis runs over, the one named last changes fastest.
Arguments:
- query_pairs: bfloat16 [12288, 2048], P('ep', 'tp'), may hold values from -64 to 64
- key_pairs: bfloat16 [12288, 2048], P('ep', 'tp'), may hold values from -64 to 64
- value_rows: bfloat16 [12288, 2048], P('ep', 'tp'), may hold values from -6 to 6
- head_lambda: float32 [16], P('tp'), may hold values from 0.3 to 0.8
- head_gain: float32 [128], replicated, may hold values from 0.1 to 1.9
- out_weight: bfloat16 [2048, 2048], P('tp'), may hold values from -0.1875 to 0.1875
- moe_input: bfloat16 [5120, 2048], P('ep'), may hold values from -6 to 6
- ffn_gain: float32 [2048], replicated, may hold values from 0.1 to 1.9
- routes: int32 [5120, 2], P('ep'), may hold values from 0 to 31, all different within a row; in each aligned block of 160 rows (0 to 159, 160 to 319, ...) at most 12 rows name the same one
- route_weight: float32 [5120, 2], P('ep'), may hold values from 0.25 to 2.5
- gate_weight: bfloat16 [32, 2048, 2048], P('ep', None, 'tp'), may hold values from -0.125 to 0.125
- up_weight: bfloat16 [32, 2048, 2048], P('ep', None, 'tp'), may hold values from -0.125 to 0.125
- down_weight: bfloat16 [32, 2048, 2048], P('ep', 'tp'), may hold values from -0.1875 to 0.1875
- shared_gate: bfloat16 [2048, 2048], P(None, 'tp'), may hold values from -0.125 to 0.125
- shared_up: bfloat16 [2048, 2048], P(None, 'tp'), may hold values from -0.125 to 0.125
- shared_down: bfloat16 [2048, 2048], P('tp'), may hold values from -0.1875 to 0.1875
Outputs:
- attn_out: bfloat16 [12288, 2048], P('ep', 'tp')
- moe_out: bfloat16 [5120, 2048], P('ep', 'tp')
Inputs may be any that keep to these rules, and one draw needn't show every extreme that they name: `routes`: in each aligned block of 160 rows (the rows of one device along ep) no expert is named more than 12 times, a bound that some block reaches; a row names 2 different experts.
All inputs are finite; a program needn't handle non-finite values.
Results may differ from a plain program's by a relative error of at most 0.017.
The roundings to bfloat16 on the way count: a program that leaves them out, or rounds other values in their place, can miss the bound.
Values may be sent and summed in bfloat16 or wider, within the bound.
A program may use at most 64 MiB of HBM per device.

v0:
```python
import jax
import jax.numpy as jnp
from jax import lax
from jax.sharding import PartitionSpec as P

TOP_K = 2
KEY_BLOCK = 128


theta_base = 500000.0
norm_eps = 1e-06
masked_low = -1e30


def side_by_side(arrays, axis, dim, along):
    widths = [a.shape[along] for a in arrays]
    both = jnp.concatenate(arrays, axis=along)
    out = lax.all_gather(both, axis, axis=dim, tiled=True)
    return tuple(jnp.split(out, [sum(widths[:k]) for k in range(1, len(widths))], axis=along))


def in_blocks(x, dim, peers):
    shape = x.shape
    pieces = x.reshape(*shape[:dim], peers, shape[dim] // peers, *shape[dim + 1 :])
    return jnp.moveaxis(pieces, dim, 0)


def sum_at_owner(x, axis, dim):
    peers = lax.axis_size(axis)
    pieces = lax.all_to_all(in_blocks(x, dim, peers), axis, 0, 0, tiled=True)
    return jnp.sum(pieces.astype(jnp.float32), axis=0)


def joined_along(pieces, dim):
    shape = list(pieces.shape[1:])
    shape[dim] *= pieces.shape[0]
    return jnp.moveaxis(pieces, 0, dim).reshape(shape)


def copy_for_each(x, axis):
    copies = jnp.broadcast_to(x, (lax.axis_size(axis), *x.shape))
    return lax.all_to_all(copies, axis, split_axis=0, concat_axis=0, tiled=True)


def gather_directly(x, axis, dim):
    return joined_along(copy_for_each(x, axis), dim)


def sent_together(arrays, axis, dim, along):
    both = jnp.concatenate(arrays, axis=along)
    out, at, finished = (sum_at_owner(both, axis, dim), 0, [])
    for a in arrays:
        finished.append(lax.slice_in_dim(out, at, at + a.shape[along], axis=along))
        at += a.shape[along]
    return tuple(finished)


def rotate(inputs, positions):
    half_size = inputs.shape[-1] // 2
    frequency = theta_base ** (-(jnp.arange(half_size, dtype=jnp.float32) * 2.0) / inputs.shape[-1])
    angles = positions.astype(jnp.float32)[:, None] * frequency[None, :]
    cosine = jnp.cos(angles)[:, None, None, :]
    sine_part = jnp.sin(angles)[:, None, None, :]
    front_half = inputs[..., :half_size]
    back_half = inputs[..., half_size:]
    return jnp.concatenate(
        [front_half * cosine - back_half * sine_part, back_half * cosine + front_half * sine_part],
        axis=-1,
    )


def local(
    query_pairs,
    key_pairs,
    value_rows,
    head_lambda,
    head_gain,
    out_weight,
    moe_input,
    ffn_gain,
    routes,
    route_weight,
    gate_weight,
    up_weight,
    down_weight,
    shared_gate,
    shared_up,
    shared_down,
):
    local_rows = query_pairs.shape[0]
    local_heads = head_lambda.shape[0]
    head_size = query_pairs.shape[1] // (2 * local_heads)
    value_size = value_rows.shape[1] // local_heads
    positions = lax.axis_index("ep") * local_rows + jnp.arange(local_rows, dtype=jnp.int32)
    rot_queries = rotate(
        query_pairs.astype(jnp.float32).reshape(local_rows, local_heads, 2, head_size), positions
    ).astype(jnp.bfloat16)
    rot_keys = rotate(
        key_pairs.astype(jnp.float32).reshape(local_rows, local_heads, 2, head_size), positions
    ).astype(jnp.bfloat16)
    rot_keys = rot_keys.reshape(local_rows, local_heads * 2 * head_size)
    zero_init = (
        jnp.full((local_heads, 2, local_rows), masked_low, jnp.float32),
        jnp.zeros((local_heads, 2, local_rows), jnp.float32),
        jnp.zeros((local_heads, 2, local_rows, value_size), jnp.float32),
    )
    piece_keys, piece_values = side_by_side((rot_keys, value_rows), "ep", 0, 1)
    block_count = piece_keys.shape[0] // KEY_BLOCK
    group_size = 4
    group_count = block_count // group_size
    grouped_keys = piece_keys.reshape(group_count, group_size, KEY_BLOCK, local_heads, 2, head_size)
    grouped_values = piece_values.reshape(
        group_count, group_size, KEY_BLOCK, local_heads, value_size
    )

    def one_group(current, inputs):
        block_keys, block_values, group_index = inputs
        key_positions = group_index * group_size * KEY_BLOCK + jnp.arange(
            group_size * KEY_BLOCK, dtype=jnp.int32
        ).reshape(group_size, KEY_BLOCK)
        scores = jnp.einsum(
            "qhmd,gkhmd->hmqgk", rot_queries, block_keys, preferred_element_type=jnp.float32
        ) * head_size ** (-0.5)
        allowed = key_positions[None, :, :] <= positions[:, None, None]
        scores = jnp.where(allowed, scores, masked_low)
        block_max = jnp.max(scores, axis=-1)
        weights = jnp.where(allowed, jnp.exp(scores - block_max[..., None]), 0.0)
        block_sum = jnp.sum(weights, axis=-1)
        block_out = jnp.einsum(
            "hmqgk,gkhc->hmqgc",
            weights.astype(jnp.bfloat16),
            block_values,
            preferred_element_type=jnp.float32,
        )
        run_max, run_sum, run_out = current
        new_max = jnp.maximum(run_max, jnp.max(block_max, axis=-1))
        old_scale = jnp.exp(run_max - new_max)
        new_scale = jnp.exp(block_max - new_max[..., None])
        run_sum = run_sum * old_scale + jnp.sum(new_scale * block_sum, axis=-1)
        run_out = run_out * old_scale[..., None] + jnp.sum(
            new_scale[..., None] * block_out, axis=-2
        )
        return ((new_max, run_sum, run_out), None)

    result, _ = lax.scan(
        one_group,
        zero_init,
        (grouped_keys, grouped_values, jnp.arange(group_count, dtype=jnp.int32)),
    )
    run_max, run_sum, run_out = result
    map_outputs = run_out / run_sum[..., None]
    difference = map_outputs[:, 0] - head_lambda[:, None, None] * map_outputs[:, 1]
    inverse_rms = lax.rsqrt(jnp.mean(difference * difference, axis=-1, keepdims=True) + norm_eps)
    normed_heads = (difference * inverse_rms * head_gain).astype(jnp.bfloat16)
    head_rows = normed_heads.transpose(1, 0, 2).reshape(local_rows, local_heads * value_size)
    mixer_terms = jnp.dot(head_rows, out_weight, preferred_element_type=jnp.float32)
    attn_out = sum_at_owner(mixer_terms.astype(jnp.bfloat16), "tp", 1).astype(jnp.bfloat16)
    row_values = moe_input.astype(jnp.float32)
    inverse_norm = lax.rsqrt(jnp.mean(row_values * row_values, axis=-1, keepdims=True) + norm_eps)
    normed = (row_values * inverse_norm * ffn_gain).astype(jnp.bfloat16)
    token_rows = normed.shape[0]
    experts = lax.axis_size("ep")
    capacity = token_rows * TOP_K * 5 // (4 * experts)
    flat_routes = routes.reshape(-1)
    onehot = (flat_routes[:, None] == jnp.arange(experts, dtype=jnp.int32)).astype(jnp.int32)
    slot_rank = jnp.sum((jnp.cumsum(onehot, axis=0) - 1) * onehot, axis=-1)
    slot_index = flat_routes * capacity + slot_rank
    token_index = jnp.arange(token_rows * TOP_K, dtype=jnp.int32) // TOP_K
    slot_rows = (
        jnp.full((experts * capacity,), token_rows, jnp.int32).at[slot_index].set(token_index)
    )
    padded = jnp.concatenate([normed, jnp.zeros((1, normed.shape[1]), jnp.bfloat16)], axis=0)
    column_width = normed.shape[1] // lax.axis_size("tp")
    padded_cols = lax.dynamic_slice_in_dim(
        padded, lax.axis_index("tp") * column_width, column_width, 1
    )
    outgoing = padded_cols[slot_rows]
    arrived = lax.all_to_all(outgoing, "ep", split_axis=0, concat_axis=0, tiled=True)
    pieces = gather_directly(arrived, "tp", 1)
    gate_rows = gate_weight[0]
    up_rows = up_weight[0]
    gate_part = jnp.dot(pieces, gate_rows, preferred_element_type=jnp.float32)
    up_part = jnp.dot(pieces, up_rows, preferred_element_type=jnp.float32)
    hidden = (jax.nn.silu(gate_part) * up_part).astype(jnp.bfloat16)
    expert_terms = jnp.dot(hidden, down_weight[0], preferred_element_type=jnp.float32)
    shared_gated = jnp.dot(normed, shared_gate, preferred_element_type=jnp.float32)
    shared_lifted = jnp.dot(normed, shared_up, preferred_element_type=jnp.float32)
    shared_hidden = (jax.nn.silu(shared_gated) * shared_lifted).astype(jnp.bfloat16)
    shared_terms = jnp.dot(shared_hidden, shared_down, preferred_element_type=jnp.float32)
    expert_sum, shared_sum = sent_together(
        (expert_terms.astype(jnp.bfloat16), shared_terms.astype(jnp.bfloat16)), "tp", 1, 0
    )
    returned = lax.all_to_all(
        expert_sum.astype(jnp.bfloat16), "ep", split_axis=0, concat_axis=0, tiled=True
    )
    picked = returned[slot_index.reshape(token_rows, TOP_K)]
    moe_out = (
        jnp.sum(route_weight[..., None] * picked.astype(jnp.float32), axis=1) + shared_sum
    ).astype(jnp.bfloat16)
    return (attn_out, moe_out)


def solution(mesh):
    return jax.shard_map(
        local,
        mesh=mesh,
        in_specs=(
            P("ep", "tp"),
            P("ep", "tp"),
            P("ep", "tp"),
            P("tp"),
            P(),
            P("tp", None),
            P("ep", None),
            P(),
            P("ep", None),
            P("ep", None),
            P("ep", None, "tp"),
            P("ep", None, "tp"),
            P("ep", "tp", None),
            P(None, "tp"),
            P(None, "tp"),
            P("tp", None),
        ),
        out_specs=(P("ep", "tp"), P("ep", "tp")),
        check_vma=False,
    )
```

profile of v0, /device:TPU:1, one launch (start us, length us, event | category | flops | bytes accessed | tf_op | source)
XLA Modules:
  0.0 315.2 jit_solution(545244832504321701)
XLA Ops:
  14.6 2.9 scatter_custom_fusion
  18.0 1.4 gather_fusion
  19.5 34.3 %all_to_all.39 = bf16[32,12,128]{2,1,0:T(8,128)(2,1)S(1)} all-to-all(bf16[32,12,128]{2,1,0:T(8,128)(2,1)S(1)} %all_to_all.26), channel_id=1, replica_groups=mesh['ep'=32,'tp'=16] {'ep'}, dimensions={0} | all-to-all | bytes 196608 | tf_op jit(solution)/shard_map/all_to_all | solution.py:178
  54.0 1.4 broadcast_in_dim.37
  55.4 6.7 %all-to-all-start.2 = ((bf16[16,384,128]{1,2,0:T(8,128)(2,1)}), bf16[16,384,128]{1,2,0:T(8,128)(2,1)S(1)}, u32[]{:S(2)}, u32[]{:S(2)}) async-start(bf16[16,384,128]{1,2,0:T(8,128)(2,1)} %broadcast_in_dim.37), calls=%async_computation.2 | async-start | bytes 3145728 | tf_op jit(solution)/shard_map/all_to_all | solution.py:42
  62.4 1.8 convolution_convert_fusion.2
  64.2 19.0 %all-to-all-done.2 = bf16[16,384,128]{1,2,0:T(8,128)(2,1)S(1)} async-done(((bf16[16,384,128]{1,2,0:T(8,128)(2,1)}), bf16[16,384,128]{1,2,0:T(8,128)(2,1)S(1)}, u32[]{:S(2)}, u32[]{:S(2)}) %all-to-all-start.2) | async-done | bytes 1572896 | tf_op jit(solution)/shard_map/all_to_all | solution.py:42
  83.2 1.6 fusion.20
  84.9 4.1 %convolution_convert_fusion = bf16[384,2048]{1,0:T(8,128)(2,1)} fusion(bf16[384,2048]{0,1:T(8,128)(2,1)S(1)} %bitcast.127, bf16[1,128,2048]{2,1,0:T(8,128)(2,1)S(1)} %copy-done, bf16[1,2048,128]{2,1,0:T(8,128)(2,1)} %param.29, f32[384,128]{1,0:T(8,128)S(1)} %fusion.20), kind=kOutput, calls=%fused_computation.31 | convolution fusion | flops 403734528 | bytes 4390912 | tf_op jit(solution)/shard_map/dot_general | solution.py:185
  89.0 3.2 %bitcast_bitcast_fusion = bf16[16,544,128]{2,1,0:T(8,128)(2,1)} fusion(bf16[160,2048]{1,0:T(8,128)(2,1)S(1)} %convolution_convert_fusion.2, bf16[384,2048]{1,0:T(8,128)(2,1)} %convolution_convert_fusion), kind=kLoop, calls=%fused_computation.34 | loop fusion | flops 4456448 | bytes 4456448 | tf_op jit(solution)/shard_map/transpose | solution.py:25
  92.1 6.2 %all-to-all-start.3 = ((bf16[16,544,128]{2,1,0:T(8,128)(2,1)}), bf16[16,544,128]{2,1,0:T(8,128)(2,1)S(1)}, u32[]{:S(2)}, u32[]{:S(2)}) async-start(bf16[16,544,128]{2,1,0:T(8,128)(2,1)} %bitcast_bitcast_fusion), calls=%async_computation.3 | async-start | bytes 4456448 | tf_op jit(solution)/shard_map/all_to_all | solution.py:30
  99.0 30.9 %all-to-all-done.3 = bf16[16,544,128]{2,1,0:T(8,128)(2,1)S(1)} async-done(((bf16[16,544,128]{2,1,0:T(8,128)(2,1)}), bf16[16,544,128]{2,1,0:T(8,128)(2,1)S(1)}, u32[]{:S(2)}, u32[]{:S(2)}) %all-to-all-start.3) | async-done | bytes 2228256 | tf_op jit(solution)/shard_map/all_to_all | solution.py:30
  130.9 8.0 %all-to-all-start.4 = ((bf16[32,12,128]{2,1,0:T(8,128)(2,1)}), bf16[32,12,128]{2,1,0:T(8,128)(2,1)S(1)}, u32[]{:S(2)}, u32[]{:S(2)}) async-start(bf16[32,12,128]{2,1,0:T(8,128)(2,1)} %all_to_all.31), calls=%async_computation.4 | async-start | bytes 262144 | tf_op jit(solution)/shard_map/all_to_all | solution.py:193
  139.0 6.2 %fusion.54 = (bf16[12288,128]{0,1:T(8,128)(2,1)}, bf16[12288,128]{0,1:T(8,128)(2,1)}) fusion(bf16[12288,256]{0,1:T(8,128)(2,1)} %all-gather.2.cloned.1.call-done), kind=kLoop, calls=%fused_computation.120 | loop fusion | bytes 12582912 | tf_op jit(solution)/shard_map/split | solution.py:19
  145.2 4.6 %copy.57 = bf16[12288,128]{1,0:T(8,128)(2,1)} copy(bf16[12288,128]{0,1:T(8,128)(2,1)} %get-tuple-element.205) | data formatting | bytes 6291456 | tf_op jit(solution)/shard_map/split | solution.py:19
  149.8 7.4 %reshape.373 = bf16[24,4,128,1,2,64]{2,1,0,5,4,3:T(4,128)(2,1)} reshape(bf16[12288,128]{0,1:T(8,128)(2,1)} %get-tuple-element.206) | data formatting | bytes 6291456 | tf_op jit(solution)/shard_map/reshape | solution.py:111
  157.2 119.2 %while.17 = (s32[]{:T(128)}, f32[1,2,384]{2,1,0:T(2,128)S(1)}, f32[1,2,384]{2,1,0:T(2,128)S(1)}, f32[1,2,384,128]{2,3,1,0:T(8,128)S(1)}, s32[24]{0:T(128)S(1)}, ...) while((s32[]{:T(128)}, f32[1,2,384]{2,1,0:T(2,128)S(1)}, ...), condition=%wide.region_6.7_spmd.clone, body=%wide.region_0.6_spmd.clone.sunk | while | flops 155329920 | bytes 7668389 | solution.py:145
  160.7 1.3 fusion.75
  170.6 1.3 fusion.75
  175.6 1.3 fusion.75
  277.2 1.6 copy.88
  278.8 3.8 %all-to-all-start = ((bf16[16,384,128]{2,1,0:T(8,128)(2,1)}), bf16[16,384,128]{2,1,0:T(8,128)(2,1)S(1)}, u32[]{:S(2)}, u32[]{:S(2)}) async-start(bf16[16,384,128]{2,1,0:T(8,128)(2,1)} %bitcast.104), calls=%async_computation | async-start | bytes 3145728 | tf_op jit(solution)/shard_map/all_to_all | solution.py:30
  283.0 1.4 gather_fusion.1
  285.3 22.2 %all-to-all-done = bf16[16,384,128]{2,1,0:T(8,128)(2,1)S(1)} async-done(((bf16[16,384,128]{2,1,0:T(8,128)(2,1)}), bf16[16,384,128]{2,1,0:T(8,128)(2,1)S(1)}, u32[]{:S(2)}, u32[]{:S(2)}) %all-to-all-start) | async-done | bytes 1572896 | tf_op jit(solution)/shard_map/all_to_all | solution.py:30
  (408 shorter events, 109.5 us)
Async XLA Ops:
  7.2 77.7 %copy-start = (bf16[1,128,2048]{2,1,0:T(8,128)(2,1)S(1)}, bf16[1,128,2048]{2,1,0:T(8,128)(2,1)}, u32[]{:S(2)}) copy-start(bf16[1,128,2048]{2,1,0:T(8,128)(2,1)} %param.30) | copy-start | bytes 1572868
  7.2 4.9 %copy-start.7 = (s32[160,2]{0,1:T(2,128)S(1)}, s32[160,2]{0,1:T(2,128)}, u32[]{:S(2)}) copy-start(s32[160,2]{0,1:T(2,128)} %param.26) | copy-start | bytes 3844
  7.2 131.8 %all-gather.2.cloned.1.call-start = ((), (), s32[]{:S(2)}) async-start(), calls=%async_computation.5 | async-start | bytes 6488064 | tf_op jit(solution)/shard_map/all_gather | solution.py:18
  9.3 8.3 %copy-start.1 = (bf16[160,2048]{1,0:T(8,128)(2,1)S(1)}, bf16[160,2048]{1,0:T(8,128)(2,1)}, u32[]{:S(2)}) copy-start(bf16[160,2048]{1,0:T(8,128)(2,1)} %param.24) | copy-start | bytes 1966084
  10.6 7.2 %copy-start.6 = (f32[2048]{0:T(1024)S(1)}, f32[2048]{0:T(1024)}, u32[]{:S(2)}) copy-start(f32[2048]{0:T(1024)} %param.25) | copy-start | bytes 24580
  55.3 6.7 %copy-start.3 = (bf16[2048,128]{1,0:T(8,128)(2,1)S(1)}, bf16[2048,128]{1,0:T(8,128)(2,1)}, u32[]{:S(2)}) copy-start(bf16[2048,128]{1,0:T(8,128)(2,1)} %param.31) | copy-start | bytes 1572868
  55.4 27.9 %all-to-all-start.2 = ((bf16[16,384,128]{1,2,0:T(8,128)(2,1)}), bf16[16,384,128]{1,2,0:T(8,128)(2,1)S(1)}, u32[]{:S(2)}, u32[]{:S(2)}) async-start(bf16[16,384,128]{1,2,0:T(8,128)(2,1)} %broadcast_in_dim.37), calls=%async_computation.2 | async-start | bytes 3145728 | tf_op jit(solution)/shard_map/all_to_all | solution.py:42
  92.1 37.7 %all-to-all-start.3 = ((bf16[16,544,128]{2,1,0:T(8,128)(2,1)}), bf16[16,544,128]{2,1,0:T(8,128)(2,1)S(1)}, u32[]{:S(2)}, u32[]{:S(2)}) async-start(bf16[16,544,128]{2,1,0:T(8,128)(2,1)} %bitcast_bitcast_fusion), calls=%async_computation.3 | async-start | bytes 4456448 | tf_op jit(solution)/shard_map/all_to_all | solution.py:30
  130.9 147.9 %all-to-all-start.4 = ((bf16[32,12,128]{2,1,0:T(8,128)(2,1)}), bf16[32,12,128]{2,1,0:T(8,128)(2,1)S(1)}, u32[]{:S(2)}, u32[]{:S(2)}) async-start(bf16[32,12,128]{2,1,0:T(8,128)(2,1)} %all_to_all.31), calls=%async_computation.4 | async-start | bytes 262144 | tf_op jit(solution)/shard_map/all_to_all | solution.py:193
  149.8 7.4 %copy-start.5 = (bf16[384,1,2,64]{0,3,2,1:T(8,128)(2,1)S(1)}, bf16[384,1,2,64]{0,3,2,1:T(8,128)(2,1)}, u32[]{:S(2)}) copy-start(bf16[384,1,2,64]{0,3,2,1:T(8,128)(2,1)} %get-tuple-element.298) | copy-start | bytes 294916
  157.2 119.3 %copy-start.2 = (bf16[128,2048]{1,0:T(8,128)(2,1)S(1)}, bf16[128,2048]{1,0:T(8,128)(2,1)}, u32[]{:S(2)}) copy-start(bf16[128,2048]{1,0:T(8,128)(2,1)} %param.23) | copy-start | bytes 1572868
  157.2 119.3 %copy-start.9 = (f32[128]{0:T(128)S(1)}, f32[128]{0:T(128)}, u32[]{:S(2)}) copy-start(f32[128]{0:T(128)} %param.22) | copy-start | bytes 1540
  278.8 3.9 %copy-start.4 = (s32[160,2]{1,0:T(8,128)S(1)}, s32[160,2]{1,0:T(8,128)}, u32[]{:S(2)}) copy-start(s32[160,2]{1,0:T(8,128)} %get-tuple-element.213) | copy-start | bytes 3844
  278.8 4.0 %copy-start.8 = (f32[160,2]{0,1:T(2,128)S(1)}, f32[160,2]{0,1:T(2,128)}, u32[]{:S(2)}) copy-start(f32[160,2]{0,1:T(2,128)} %param.27) | copy-start | bytes 3844
  278.8 28.7 %all-to-all-start = ((bf16[16,384,128]{2,1,0:T(8,128)(2,1)}), bf16[16,384,128]{2,1,0:T(8,128)(2,1)S(1)}, u32[]{:S(2)}, u32[]{:S(2)}) async-start(bf16[16,384,128]{2,1,0:T(8,128)(2,1)} %bitcast.104), calls=%async_computation | async-start | bytes 3145728 | tf_op jit(solution)/shard_map/all_to_all | solution.py:30
Sparse Core Ops, SparseCore 0:
  12.2 86.2 all-gather.1
where the time goes:
time: 317 us; the launch traced here: 315 us
  waiting for transfers between devices  72.1 us (23%)
  local copies, waits for them, and re-layouts  69.2 us (22%)
  matrix products  53.2 us (17%)
  blocking collectives  34.3 us (11%)
  other arithmetic  28.6 us (9%)
  starting transfers between devices  24.8 us (8%)
  loops' own time  17.8 us (6%)
  between operations  15.1 us (5%)
    all_to_all x2, waiting for transfers between devices, sum_at_owner(): pieces = lax.all_to_all(in_blocks(x, dim, peers), axis, 0, 0, tiled=True)  53.1 us
    dynamic_slice x48, local copies, waits for them, and re-layouts, local(): lax.scan(one_group, zero_init, (grouped_keys, grouped_values, jnp.arange(...  37.1 us
    all_to_all x1, blocking collectives, local(): lax.all_to_all(outgoing, 'ep', split_axis=0, concat_axis=0, tiled=True)  34.3 us
    dot_general x24, matrix products, one_group(): jnp.einsum('hmqgk,gkhc->hmqgc', weights.astype(jnp.bfloat16), block_value...  32.3 us
    all_to_all x1, waiting for transfers between devices, copy_for_each(): return lax.all_to_all(copies, axis, split_axis=0, concat_axis=0, tiled=True)  19 us
    another operation x1, loops' own time, local(): lax.scan(one_group, zero_init, (grouped_keys, grouped_values, jnp.arange(...  17.8 us
    dot_general x24, matrix products, one_group(): jnp.einsum('qhmd,gkhmd->hmqgk', rot_queries, block_keys, preferred_elemen...  12.3 us
    split x2, local copies, waits for them, and re-layouts, side_by_side(): jnp.split(out, [sum(widths[:k]) for k in range(1, len(widths))], axis=along)  10.8 us
  transfers between devices with their start and end apart: 5, of which 3 were waited for; matrix products, arithmetic and copies ran while one was open for 46% of the time, Pallas kernels for 0%

commit v1 on v0

v1 whole, which is shorter than its diff:
```python
import functools

import jax
import jax.numpy as jnp
from jax import lax
from jax.experimental import pallas as pl
from jax.experimental.pallas import tpu as pltpu
from jax.sharding import PartitionSpec as P

TOP_K = 2

theta_base = 500000.0
norm_eps = 1e-06
masked_low = -1e30

CORES = 2
LANES = 128
MESH = pl.DeviceIdType.MESH
f32 = jnp.float32
bf16 = jnp.bfloat16


def rotation_tables(rows):
    shape = (rows, LANES)
    lane = lax.broadcasted_iota(jnp.int32, shape, 1)
    place = (lane % 32).astype(f32)
    frequency = theta_base ** (-(place * 2.0) / 64)
    positions = lax.axis_index("ep") * rows + lax.broadcasted_iota(jnp.int32, shape, 0)
    angles = positions.astype(f32) * frequency
    sign = jnp.where(lane % 64 < 32, -1.0, 1.0)
    return jnp.cos(angles), jnp.sin(angles) * sign


def rotated(x, cosine, sine):
    x = x.astype(f32)
    lane = lax.broadcasted_iota(jnp.int32, x.shape, 1)
    swapped = jnp.where(lane % 64 < 32, pltpu.roll(x, 96, 1), pltpu.roll(x, 32, 1))
    return x * cosine + swapped * sine


def split_tp(nx):
    tp = lax.axis_index("tp")
    return tp // nx, tp % nx


class Projection:
    def __init__(self, ny, nx, rows, w_hbm, wb, hx, pr, rr, sems):
        self.ny, self.nx, self.rows = ny, nx, rows
        self.w, self.wb, self.hx, self.pr, self.rr = w_hbm, wb, hx, pr, rr
        self.w_send, self.w_recv, self.w_local, self.h_send, self.h_recv, self.p_send, self.p_recv = sems
        self.y, self.x = split_tp(nx)
        self.ep = lax.axis_index("ep")

    def _device(self, y, x):
        return (self.ep, y * self.nx + x)

    def _weight(self, i):
        y = lax.rem(self.y + i, self.ny)
        width = self.nx * LANES
        cols = pl.ds(pl.multiple_of(y * width, width), width)
        rows = pl.ds(pl.multiple_of(self.y * LANES, LANES), LANES)
        return pltpu.make_async_remote_copy(
            src_ref=self.w.at[:, cols],
            dst_ref=self.wb.at[rows, :],
            send_sem=self.w_send.at[i],
            recv_sem=self.w_recv.at[i],
            device_id=self._device(y, self.x),
            device_id_type=MESH,
        )

    def _weight_own(self):
        width = self.nx * LANES
        cols = pl.ds(pl.multiple_of(self.y * width, width), width)
        rows = pl.ds(pl.multiple_of(self.y * LANES, LANES), LANES)
        return pltpu.make_async_copy(self.w.at[:, cols], self.wb.at[rows, :], self.w_local)

    def start_weights(self):
        self._weight_own().start()
        for i in range(1, self.ny):
            self._weight(i).start()

    def _gather(self, i):
        y = lax.rem(self.y + i, self.ny)
        cols = pl.ds(pl.multiple_of(self.y * LANES, LANES), LANES)
        return pltpu.make_async_remote_copy(
            src_ref=self.hx.at[:, cols],
            dst_ref=self.hx.at[:, cols],
            send_sem=self.h_send.at[i],
            recv_sem=self.h_recv.at[i],
            device_id=self._device(y, self.x),
            device_id_type=MESH,
        )

    def start_gather(self, h):
        cols = pl.ds(pl.multiple_of(self.y * LANES, LANES), LANES)
        self.hx[:, cols] = h
        for i in range(1, self.ny):
            self._gather(i).start()

    def _partial(self, i):
        x = lax.rem(self.x + i, self.nx)
        return pltpu.make_async_remote_copy(
            src_ref=self.pr.at[i],
            dst_ref=self.rr.at[i],
            send_sem=self.p_send.at[i],
            recv_sem=self.p_recv.at[i],
            device_id=self._device(self.y, x),
            device_id_type=MESH,
        )

    def multiply_and_send(self):
        self._weight_own().wait()
        for i in range(1, self.ny):
            self._weight(i).wait()
        for i in range(1, self.ny):
            self._gather(i).wait()
        h = self.hx[...]
        for i in list(range(1, self.nx)) + [0]:
            x = lax.rem(self.x + i, self.nx)
            w = self.wb[:, pl.ds(pl.multiple_of(x * LANES, LANES), LANES)]
            self.pr[i] = jnp.dot(h, w, preferred_element_type=f32).astype(bf16)
            if i:
                self._partial(i).start()

    def finish(self):
        for i in range(1, self.nx):
            self._partial(i).wait()
        total = self.pr[0].astype(f32)
        for i in range(1, self.nx):
            total = total + self.rr[i].astype(f32)
        return total


class Ring:
    def __init__(self, nz, kbuf, vbuf, recv, send, pass_send):
        self.nz = nz
        self.up_steps, self.down_steps = nz // 2, nz - 1 - nz // 2
        self.bufs = (kbuf, vbuf)
        self.recv, self.send, self.pass_send = recv, send, pass_send
        ep = lax.axis_index("ep")
        self.tp = lax.axis_index("tp")
        self.z, self.c = ep // CORES, ep % CORES

    def _device(self, z, c):
        return (z * CORES + c, self.tp)

    def neighbours(self):
        up = lax.rem(self.z + 1, self.nz)
        down = lax.rem(self.z + self.nz - 1, self.nz)
        return [self._device(up, self.c), self._device(down, self.c), self._device(self.z, 1 - self.c)]

    def copy(self, source, part, to_z, sem):
        slot = source * CORES + self.c
        ref = self.bufs[part].at[slot]
        return pltpu.make_async_remote_copy(
            src_ref=ref,
            dst_ref=ref,
            send_sem=self.send.at[sem, part],
            recv_sem=self.recv.at[slot, part],
            device_id=self._device(to_z, self.c),
            device_id_type=MESH,
        )

    def up(self, source, part):
        return self.copy(source, part, lax.rem(self.z + 1, self.nz), source)

    def down(self, source, part, sem=None):
        to = lax.rem(self.z + self.nz - 1, self.nz)
        return self.copy(source, part, to, source if sem is None else sem)

    def handed(self, source, part, core):
        slot = source * CORES + core
        ref = self.bufs[part].at[slot]
        return pltpu.make_async_remote_copy(
            src_ref=ref,
            dst_ref=ref,
            send_sem=self.pass_send.at[source, part],
            recv_sem=self.recv.at[slot, part],
            device_id=self._device(self.z, 1 - self.c),
            device_id_type=MESH,
        )

    def up_source(self, t):
        return self.z - t, self.z - t >= 0

    def down_source(self, t):
        source = lax.rem(self.z + t, self.nz)
        return source, jnp.logical_and(source < self.down_steps, t <= self.down_steps)

    def start_own(self):
        for part in range(2):

            @pl.when(self.z < self.nz - 1)
            def _():
                self.up(self.z, part).start()

            @pl.when(self.z < self.down_steps)
            def _():
                self.down(self.z, part, self.nz).start()

            @pl.when(self.c == 0)
            def _():
                self.handed(self.z, part, self.c).start()

    def serve(self, t, part):
        source, here = self.up_source(t)

        @pl.when(here)
        def _():
            self.up(source, part).wait_recv()

            @pl.when(jnp.logical_and(t < self.up_steps, self.z < self.nz - 1))
            def _():
                self.up(source, part).start()

            self.handed(source, part, self.c).start()

        source_d, here_d = self.down_source(t)

        @pl.when(here_d)
        def _():
            self.down(source_d, part).wait_recv()

            @pl.when(t < self.down_steps)
            def _():
                self.down(source_d, part).start()

            @pl.when(source_d < self.z)
            def _():
                self.handed(source_d, part, self.c).start()

    def wait_handed(self, source):
        for part in range(2):
            self.handed(source, part, 1 - self.c).wait_recv()

    def wait_sends(self):
        for part in range(2):

            @pl.when(self.z < self.nz - 1)
            def _():
                self.up(self.z, part).wait_send()

            @pl.when(self.z < self.down_steps)
            def _():
                self.down(self.z, part, self.nz).wait_send()

            @pl.when(self.c == 0)
            def _():
                self.handed(self.z, part, self.c).wait_send()

        @pl.loop(1, self.up_steps + 1)
        def _(t):
            source, here = self.up_source(t)
            source_d, here_d = self.down_source(t)

            @pl.when(here)
            def _():
                for part in range(2):
                    self.handed(source, part, self.c).wait_send()

                    @pl.when(jnp.logical_and(t < self.up_steps, self.z < self.nz - 1))
                    def _():
                        self.up(source, part).wait_send()

            @pl.when(here_d)
            def _():
                for part in range(2):

                    @pl.when(t < self.down_steps)
                    def _():
                        self.down(source_d, part).wait_send()

                    @pl.when(source_d < self.z)
                    def _():
                        self.handed(source_d, part, self.c).wait_send()


class Softmax:
    def __init__(self, rows, tile, qz, kbuf, vbuf, top, total, acc):
        self.rows, self.tile = rows, tile
        self.qz, self.kbuf, self.vbuf = qz, kbuf, vbuf
        self.top, self.total, self.acc = top, total, acc

    def _tiles(self):
        return [pl.ds(i * self.tile, self.tile) for i in range(2 * self.rows // self.tile)]

    def diagonal(self, slot):
        keys, values = self.kbuf[slot], self.vbuf[slot]
        for i, rows in enumerate(self._tiles()):
            s = lax.dot_general(self.qz[rows, :], keys, (((1,), (1,)), ((), ())), preferred_element_type=f32)
            row = i * self.tile + lax.broadcasted_iota(jnp.int32, s.shape, 0)
            row = jnp.where(row >= self.rows, row - self.rows, row)
            allowed = lax.broadcasted_iota(jnp.int32, s.shape, 1) <= row
            s = jnp.where(allowed, s, masked_low)
            top = jnp.max(s, axis=1, keepdims=True)
            p = jnp.where(allowed, jnp.exp(s - top), 0.0)
            self.top[rows, :] = jnp.broadcast_to(top, (self.tile, LANES))
            self.total[rows, :] = jnp.broadcast_to(jnp.sum(p, axis=1, keepdims=True), (self.tile, LANES))
            self.acc[rows, :] = jnp.dot(p.astype(bf16), values, preferred_element_type=f32)

    def _add(self, keys, values):
        for rows in self._tiles():
            s = lax.dot_general(self.qz[rows, :], keys, (((1,), (1,)), ((), ())), preferred_element_type=f32)
            before = self.top[rows, :]
            top = jnp.maximum(before, jnp.max(s, axis=1, keepdims=True))
            p = jnp.exp(s - top[:, :1])
            scale = jnp.exp(before - top)
            self.top[rows, :] = top
            self.total[rows, :] = self.total[rows, :] * scale + jnp.sum(p, axis=1, keepdims=True)
            self.acc[rows, :] = self.acc[rows, :] * scale + jnp.dot(
                p.astype(bf16), values, preferred_element_type=f32
            )

    def one(self, slot):
        self._add(self.kbuf[slot], self.vbuf[slot])

    def chip(self, source):
        pair = pl.ds(source * CORES, CORES)
        shape = (CORES * self.rows, LANES)
        self._add(self.kbuf[pair].reshape(shape), self.vbuf[pair].reshape(shape))

    def heads(self, lam, gain):
        out = self.acc[...] / self.total[...]
        diff = out[: self.rows] - lam * out[self.rows :]
        mean = jnp.mean(diff * diff, axis=1, keepdims=True)
        return (diff * lax.rsqrt(mean + norm_eps) * gain).astype(bf16)


def attention_kernel(
    dims,
    q_ref, k_ref, v_ref, cos_ref, sin_ref, lam_ref, gain_ref, w_hbm,
    out_ref,
    kbuf, vbuf, qz, top, total, acc, wb, hx, pr, rr,
    ring_recv, ring_send, pass_send, *proj_sems,
):
    nz, ny, nx, rows, tile = dims
    ep = lax.axis_index("ep")
    ring = Ring(nz, kbuf, vbuf, ring_recv, ring_send, pass_send)
    proj = Projection(ny, nx, rows, w_hbm, wb, hx, pr, rr, proj_sems)
    soft = Softmax(rows, tile, qz, kbuf, vbuf, top, total, acc)

    barrier = pltpu.get_barrier_semaphore()
    peers = ring.neighbours()
    peers += [proj._device(lax.rem(proj.y + i, ny), proj.x) for i in range(1, ny)]
    peers += [proj._device(proj.y, lax.rem(proj.x + i, nx)) for i in range(1, nx)]
    for peer in peers:
        pl.semaphore_signal(barrier, inc=1, device_id=peer, device_id_type=MESH)

    cosine, sine = cos_ref[...], sin_ref[...]
    kbuf[ep] = rotated(k_ref[...], cosine, sine).astype(bf16)
    vbuf[ep] = v_ref[...]
    pl.semaphore_wait(barrier, len(peers))
    ring.start_own()
    proj.start_weights()

    q = rotated(q_ref[...], cosine, sine).astype(bf16).astype(f32) * 0.125
    lane = lax.broadcasted_iota(jnp.int32, q.shape, 1)
    qz[:rows, :] = jnp.where(lane < 64, q, 0.0).astype(bf16)
    qz[rows:, :] = jnp.where(lane < 64, 0.0, q).astype(bf16)
    soft.diagonal(ep)

    @pl.when(ring.c == 1)
    def _():
        ring.wait_handed(ring.z)
        soft.one(ep - 1)

    def use(source):
        ring.wait_handed(source)
        soft.chip(source)

    def use_up(t):
        source, here = ring.up_source(t)

        @pl.when(jnp.logical_and(here, t >= 1))
        def _():
            use(source)

    def use_down(t):
        source, here = ring.down_source(t)

        @pl.when(jnp.logical_and(jnp.logical_and(here, t >= 1), source < ring.z))
        def _():
            use(source)

    @pl.loop(1, ring.up_steps + 1)
    def _(t):
        ring.serve(t, 0)
        use_up(t - 1)
        ring.serve(t, 1)
        use_down(t - 1)

    use_up(ring.up_steps)
    use_down(ring.up_steps)

    proj.start_gather(soft.heads(lam_ref[0], gain_ref[...]))
    proj.multiply_and_send()
    ring.wait_sends()
    out_ref[...] = proj.finish().astype(bf16)


def attention(nz, ny, nx, query_pairs, key_pairs, value_rows, head_lambda, head_gain, out_weight):
    rows = query_pairs.shape[0]
    tile = 256 if (2 * rows) % 256 == 0 else 2 * rows
    cosine, sine = rotation_tables(rows)
    vmem = pl.BlockSpec(memory_space=pltpu.VMEM)
    slots = nz * CORES
    dma = pltpu.SemaphoreType.DMA
    return pl.pallas_call(
        functools.partial(attention_kernel, (nz, ny, nx, rows, tile)),
        out_shape=jax.ShapeDtypeStruct((rows, LANES), bf16),
        in_specs=[vmem] * 5
        + [pl.BlockSpec(memory_space=pltpu.SMEM), vmem, pl.BlockSpec(memory_space=pl.ANY)],
        out_specs=vmem,
        scratch_shapes=[
            pltpu.VMEM((slots, rows, LANES), bf16),
            pltpu.VMEM((slots, rows, LANES), bf16),
            pltpu.VMEM((2 * rows, LANES), bf16),
            pltpu.VMEM((2 * rows, LANES), f32),
            pltpu.VMEM((2 * rows, LANES), f32),
            pltpu.VMEM((2 * rows, LANES), f32),
            pltpu.VMEM((ny * LANES, nx * LANES), bf16),
            pltpu.VMEM((rows, ny * LANES), bf16),
            pltpu.VMEM((nx, rows, LANES), bf16),
            pltpu.VMEM((nx, rows, LANES), bf16),
            dma((slots, 2)),
            dma((nz + 1, 2)),
            dma((nz, 2)),
            dma((ny,)),
            dma((ny,)),
            dma(()),
            dma((ny,)),
            dma((ny,)),
            dma((nx,)),
            dma((nx,)),
        ],
        compiler_params=pltpu.CompilerParams(
            collective_id=0, has_side_effects=True, vmem_limit_bytes=56 * 1024 * 1024
        ),
        name="attention",
    )(query_pairs, key_pairs, value_rows, cosine, sine, head_lambda, head_gain.reshape(1, -1), out_weight)


def in_blocks(x, dim, peers):
    shape = x.shape
    pieces = x.reshape(*shape[:dim], peers, shape[dim] // peers, *shape[dim + 1 :])
    return jnp.moveaxis(pieces, dim, 0)


def sum_at_owner(x, axis, dim):
    peers = lax.axis_size(axis)
    pieces = lax.all_to_all(in_blocks(x, dim, peers), axis, 0, 0, tiled=True)
    return jnp.sum(pieces.astype(jnp.float32), axis=0)


def joined_along(pieces, dim):
    shape = list(pieces.shape[1:])
    shape[dim] *= pieces.shape[0]
    return jnp.moveaxis(pieces, 0, dim).reshape(shape)


def copy_for_each(x, axis):
    copies = jnp.broadcast_to(x, (lax.axis_size(axis), *x.shape))
    return lax.all_to_all(copies, axis, split_axis=0, concat_axis=0, tiled=True)


def gather_directly(x, axis, dim):
    return joined_along(copy_for_each(x, axis), dim)


def sent_together(arrays, axis, dim, along):
    both = jnp.concatenate(arrays, axis=along)
    out, at, finished = (sum_at_owner(both, axis, dim), 0, [])
    for a in arrays:
        finished.append(lax.slice_in_dim(out, at, at + a.shape[along], axis=along))
        at += a.shape[along]
    return tuple(finished)


def local(
    sizes,
    query_pairs,
    key_pairs,
    value_rows,
    head_lambda,
    head_gain,
    out_weight,
    moe_input,
    ffn_gain,
    routes,
    route_weight,
    gate_weight,
    up_weight,
    down_weight,
    shared_gate,
    shared_up,
    shared_down,
):
    attn_out = attention(*sizes, query_pairs, key_pairs, value_rows, head_lambda, head_gain, out_weight)
    row_values = moe_input.astype(jnp.float32)
    inverse_norm = lax.rsqrt(jnp.mean(row_values * row_values, axis=-1, keepdims=True) + norm_eps)
    normed = (row_values * inverse_norm * ffn_gain).astype(jnp.bfloat16)
    token_rows = normed.shape[0]
    experts = lax.axis_size("ep")
    capacity = token_rows * TOP_K * 6 // (5 * experts)
    flat_routes = routes.reshape(-1)
    onehot = (flat_routes[:, None] == jnp.arange(experts, dtype=jnp.int32)).astype(jnp.int32)
    slot_rank = jnp.sum((jnp.cumsum(onehot, axis=0) - 1) * onehot, axis=-1)
    slot_index = flat_routes * capacity + slot_rank
    token_index = jnp.arange(token_rows * TOP_K, dtype=jnp.int32) // TOP_K
    slot_rows = (
        jnp.full((experts * capacity,), token_rows, jnp.int32).at[slot_index].set(token_index)
    )
    padded = jnp.concatenate([normed, jnp.zeros((1, normed.shape[1]), jnp.bfloat16)], axis=0)
    column_width = normed.shape[1] // lax.axis_size("tp")
    padded_cols = lax.dynamic_slice_in_dim(
        padded, lax.axis_index("tp") * column_width, column_width, 1
    )
    outgoing = padded_cols[slot_rows]
    arrived = lax.all_to_all(outgoing, "ep", split_axis=0, concat_axis=0, tiled=True)
    pieces = gather_directly(arrived, "tp", 1)
    gate_rows = gate_weight[0]
    up_rows = up_weight[0]
    gate_part = jnp.dot(pieces, gate_rows, preferred_element_type=jnp.float32)
    up_part = jnp.dot(pieces, up_rows, preferred_element_type=jnp.float32)
    hidden = (jax.nn.silu(gate_part) * up_part).astype(jnp.bfloat16)
    expert_terms = jnp.dot(hidden, down_weight[0], preferred_element_type=jnp.float32)
    shared_gated = jnp.dot(normed, shared_gate, preferred_element_type=jnp.float32)
    shared_lifted = jnp.dot(normed, shared_up, preferred_element_type=jnp.float32)
    shared_hidden = (jax.nn.silu(shared_gated) * shared_lifted).astype(jnp.bfloat16)
    shared_terms = jnp.dot(shared_hidden, shared_down, preferred_element_type=jnp.float32)
    expert_sum, shared_sum = sent_together(
        (expert_terms.astype(jnp.bfloat16), shared_terms.astype(jnp.bfloat16)), "tp", 1, 0
    )
    returned = lax.all_to_all(
        expert_sum.astype(jnp.bfloat16), "ep", split_axis=0, concat_axis=0, tiled=True
    )
    picked = returned[slot_index.reshape(token_rows, TOP_K)]
    moe_out = (
        jnp.sum(route_weight[..., None] * picked.astype(jnp.float32), axis=1) + shared_sum
    ).astype(jnp.bfloat16)
    return (attn_out, moe_out)


def grid_of(mesh):
    side = int(round(mesh.shape["tp"] ** 0.5))
    return mesh.shape["ep"] // CORES, mesh.shape["tp"] // side, side


def solution(mesh):
    return jax.shard_map(
        functools.partial(local, grid_of(mesh)),
        mesh=mesh,
        in_specs=(
            P("ep", "tp"),
            P("ep", "tp"),
            P("ep", "tp"),
            P("tp"),
            P(),
            P("tp", None),
            P("ep", None),
            P(),
            P("ep", None),
            P("ep", None),
            P("ep", None, "tp"),
            P("ep", None, "tp"),
            P("ep", "tp", None),
            P(None, "tp"),
            P(None, "tp"),
            P("tp", None),
        ),
        out_specs=(P("ep", "tp"), P("ep", "tp")),
        check_vma=False,
    )
```

time: 317 us -> 192 us (0.61)
  the two profiles are of different devices: /device:TPU:1 before, /device:TPU:384 now
where the time goes in v1:
time: 192 us
  Pallas kernels  62.4 us (32%)
  waiting for transfers between devices  54.3 us (28%)
  starting transfers between devices  24 us (12%)
  blocking collectives  22 us (11%)
  local copies, waits for them, and re-layouts  10.5 us (5%)
  other arithmetic  9.19 us (5%)
  matrix products  7.76 us (4%)
    pallas_call x1, Pallas kernels, attention(): pl.pallas_call(functools.partial(attention_kernel, (nz, ny, nx, rows, til...  62.4 us
    all_to_all x1, waiting for transfers between devices, sum_at_owner(): pieces = lax.all_to_all(in_blocks(x, dim, peers), axis, 0, 0, tiled=True)  31.9 us
    all_to_all x1, waiting for transfers between devices, copy_for_each(): return lax.all_to_all(copies, axis, split_axis=0, concat_axis=0, tiled=True)  22.4 us
    all_to_all x1, blocking collectives, local(): lax.all_to_all(outgoing, 'ep', split_axis=0, concat_axis=0, tiled=True)  22 us
    all_to_all x1, starting transfers between devices, local(): lax.all_to_all(expert_sum.astype(jnp.bfloat16), 'ep', split_axis=0, conca...  13.1 us
    all_to_all x1, starting transfers between devices, copy_for_each(): return lax.all_to_all(copies, axis, split_axis=0, concat_axis=0, tiled=True)  7.17 us
    dot_general x1, matrix products, local(): jnp.dot(hidden, down_weight[0], preferred_element_type=jnp.float32)  4.01 us
  transfers between devices with their start and end apart: 3, of which 2 were waited for; matrix products, arithmetic and copies ran while one was open for 2% of the time, Pallas kernels for 33%

profile of v1, /device:TPU:384, one launch (start us, length us, event | category | flops | bytes accessed | tf_op | source)
XLA Modules:
  0.0 191.8 jit_solution(9328281591094878890)
XLA Ops:
  0.7 0.9 copy.26
  1.7 0.9 reduce-window.6
  3.1 0.7 compare_select_fusion
  4.0 2.9 %scatter_custom_fusion = s32[384]{0:T(512)S(1)} fusion(s32[320]{0:T(512)S(1)} %fusion.30, s32[320]{0:T(512)S(1)} %add_select_fusion, s32[]{:T(128)} %constant.97.clone.1), kind=kCustom, calls=%fused_computation.70 | custom fusion | bytes 1540 | tf_op jit(solution)/shard_map/scatter | solution.py:511
  6.9 1.3 fusion
  8.5 1.4 gather_fusion
  10.0 22.0 %all_to_all.34 = bf16[32,12,128]{2,1,0:T(8,128)(2,1)S(1)} all-to-all(bf16[32,12,128]{2,1,0:T(8,128)(2,1)S(1)} %all_to_all.22), channel_id=1, replica_groups=mesh['ep'=32,'tp'=16] {'ep'}, dimensions={0} | all-to-all | bytes 196608 | tf_op jit(solution)/shard_map/all_to_all | solution.py:519
  32.2 1.4 broadcast_in_dim.30
  33.5 7.2 %all-to-all-start.1 = ((bf16[16,384,128]{1,2,0:T(8,128)(2,1)}), bf16[16,384,128]{1,2,0:T(8,128)(2,1)S(1)}, u32[]{:S(2)}, u32[]{:S(2)}) async-start(bf16[16,384,128]{1,2,0:T(8,128)(2,1)} %broadcast_in_dim.30), calls=%async_computation.1 | async-start | bytes 3145728 | tf_op jit(solution)/shard_map/all_to_all | solution.py:463
  40.7 0.3 fusion.35
  41.0 1.8 convolution_convert_fusion.1
  42.8 22.4 %all-to-all-done.1 = bf16[16,384,128]{1,2,0:T(8,128)(2,1)S(1)} async-done(((bf16[16,384,128]{1,2,0:T(8,128)(2,1)}), bf16[16,384,128]{1,2,0:T(8,128)(2,1)S(1)}, u32[]{:S(2)}, u32[]{:S(2)}) %all-to-all-start.1) | async-done | bytes 1572896 | tf_op jit(solution)/shard_map/all_to_all | solution.py:463
  65.3 1.6 fusion.8
  66.9 4.0 %convolution_convert_fusion = bf16[384,2048]{1,0:T(8,128)(2,1)} fusion(bf16[384,2048]{0,1:T(8,128)(2,1)S(1)} %bitcast.44, bf16[1,128,2048]{2,1,0:T(8,128)(2,1)S(1)} %copy-done, bf16[1,2048,128]{2,1,0:T(8,128)(2,1)} %param.27, f32[384,128]{1,0:T(8,128)S(1)} %fusion.8), kind=kOutput, calls=%fused_computation.4 | convolution fusion | flops 403734528 | bytes 4390912 | tf_op jit(solution)/shard_map/dot_general | solution.py:526
  70.9 3.2 %bitcast_bitcast_fusion = bf16[16,544,128]{2,1,0:T(8,128)(2,1)} fusion(bf16[160,2048]{1,0:T(8,128)(2,1)S(1)} %convolution_convert_fusion.1, bf16[384,2048]{1,0:T(8,128)(2,1)} %convolution_convert_fusion), kind=kLoop, calls=%fused_computation.6 | loop fusion | flops 4456448 | bytes 4456448 | tf_op jit(solution)/shard_map/transpose | solution.py:446
  74.1 3.7 %all-to-all-start.2 = ((bf16[16,544,128]{2,1,0:T(8,128)(2,1)}), bf16[16,544,128]{2,1,0:T(8,128)(2,1)S(1)}, u32[]{:S(2)}, u32[]{:S(2)}) async-start(bf16[16,544,128]{2,1,0:T(8,128)(2,1)} %bitcast_bitcast_fusion), calls=%async_computation.2 | async-start | bytes 4456448 | tf_op jit(solution)/shard_map/all_to_all | solution.py:451
  77.9 31.9 %all-to-all-done.2 = bf16[16,544,128]{2,1,0:T(8,128)(2,1)S(1)} async-done(((bf16[16,544,128]{2,1,0:T(8,128)(2,1)}), bf16[16,544,128]{2,1,0:T(8,128)(2,1)S(1)}, u32[]{:S(2)}, u32[]{:S(2)}) %all-to-all-start.2) | async-done | bytes 2228256 | tf_op jit(solution)/shard_map/all_to_all | solution.py:451
  110.1 0.7 all_to_all.27
  110.8 13.1 %all-to-all-start.3 = ((bf16[32,12,128]{2,1,0:T(8,128)(2,1)}), bf16[32,12,128]{2,1,0:T(8,128)(2,1)S(1)}, u32[]{:S(2)}, u32[]{:S(2)}) async-start(bf16[32,12,128]{2,1,0:T(8,128)(2,1)} %all_to_all.27), calls=%async_computation.3 | async-start | bytes 262144 | tf_op jit(solution)/shard_map/all_to_all | solution.py:534
  124.9 1.5 select_multiply_fusion
  126.4 62.4 %attention.1 = bf16[384,128]{1,0:T(8,128)(2,1)} custom-call(bf16[384,128]{1,0:T(8,128)(2,1)} %q_ref.1, bf16[384,128]{1,0:T(8,128)(2,1)} %k_ref.1, bf16[384,128]{1,0:T(8,128)(2,1)} %v_ref.1, f32[384,128]{1,0:T(8,128)} %get-tuple-element.5.cos_ref, f32[384,128]{1,0:T(8,128)} %get-tuple-element.4.sin_ref, f32[1]{0:T(128)S(6)} %copy.39.lam_ref, ...), custom_call_target="tpu_custom_call" | custom-call | tf_op jit(solution)/shard_map/attention/pallas_call | solution.py:408
  188.8 1.4 gather_fusion.1
  190.5 0.6 fusion.18
  191.2 0.6 copy.40
  (45 shorter events, 2.2 us)
Async XLA Ops:
  0.6 66.3 %copy-start = (bf16[1,128,2048]{2,1,0:T(8,128)(2,1)S(1)}, bf16[1,128,2048]{2,1,0:T(8,128)(2,1)}, u32[]{:S(2)}) copy-start(bf16[1,128,2048]{2,1,0:T(8,128)(2,1)} %param.28) | copy-start | bytes 1572868
  0.6 7.6 %copy-start.1 = (bf16[160,2048]{1,0:T(8,128)(2,1)S(1)}, bf16[160,2048]{1,0:T(8,128)(2,1)}, u32[]{:S(2)}) copy-start(bf16[160,2048]{1,0:T(8,128)(2,1)} %param.22) | copy-start | bytes 1966084
  0.7 7.6 %copy-start.5 = (f32[2048]{0:T(1024)S(1)}, f32[2048]{0:T(1024)}, u32[]{:S(2)}) copy-start(f32[2048]{0:T(1024)} %param.23) | copy-start | bytes 24580
  33.5 7.2 %copy-start.2 = (bf16[2048,128]{1,0:T(8,128)(2,1)S(1)}, bf16[2048,128]{1,0:T(8,128)(2,1)}, u32[]{:S(2)}) copy-start(bf16[2048,128]{1,0:T(8,128)(2,1)} %param.29) | copy-start | bytes 1572868
  33.5 31.7 %all-to-all-start.1 = ((bf16[16,384,128]{1,2,0:T(8,128)(2,1)}), bf16[16,384,128]{1,2,0:T(8,128)(2,1)S(1)}, u32[]{:S(2)}, u32[]{:S(2)}) async-start(bf16[16,384,128]{1,2,0:T(8,128)(2,1)} %broadcast_in_dim.30), calls=%async_computation.1 | async-start | bytes 3145728 | tf_op jit(solution)/shard_map/all_to_all | solution.py:463
  74.1 35.7 %all-to-all-start.2 = ((bf16[16,544,128]{2,1,0:T(8,128)(2,1)}), bf16[16,544,128]{2,1,0:T(8,128)(2,1)S(1)}, u32[]{:S(2)}, u32[]{:S(2)}) async-start(bf16[16,544,128]{2,1,0:T(8,128)(2,1)} %bitcast_bitcast_fusion), calls=%async_computation.2 | async-start | bytes 4456448 | tf_op jit(solution)/shard_map/all_to_all | solution.py:451
  77.9 46.1 %copy-start.4 = (s32[160,2]{1,0:T(8,128)S(1)}, s32[160,2]{1,0:T(8,128)}, u32[]{:S(2)}) copy-start(s32[160,2]{1,0:T(8,128)} %get-tuple-element.2) | copy-start | bytes 3844
  77.9 46.2 %copy-start.6 = (f32[160,2]{0,1:T(2,128)S(1)}, f32[160,2]{0,1:T(2,128)}, u32[]{:S(2)}) copy-start(f32[160,2]{0,1:T(2,128)} %param.25) | copy-start | bytes 3844
  110.8 78.0 %all-to-all-start.3 = ((bf16[32,12,128]{2,1,0:T(8,128)(2,1)}), bf16[32,12,128]{2,1,0:T(8,128)(2,1)S(1)}, u32[]{:S(2)}, u32[]{:S(2)}) async-start(bf16[32,12,128]{2,1,0:T(8,128)(2,1)} %all_to_all.27), calls=%async_computation.3 | async-start | bytes 262144 | tf_op jit(solution)/shard_map/all_to_all | solution.py:534
  188.8 2.4 %copy-start.3 = (bf16[384,128]{1,0:T(8,128)(2,1)S(1)}, bf16[384,128]{1,0:T(8,128)(2,1)}, u32[]{:S(2)}) copy-start(bf16[384,128]{1,0:T(8,128)(2,1)} %attention.1) | copy-start | bytes 294916

commit v2 on v1

--- a/solution.py
+++ b/solution.py
@@ -15,9 +15,13 @@
 
 CORES = 2
 LANES = 128
+PAD = 16
 MESH = pl.DeviceIdType.MESH
 f32 = jnp.float32
 bf16 = jnp.bfloat16
+
+AXES = ("y", "x", "x")
+SPREAD_AT, SHARED_AT, EXPERT_AT = 2, 3, 6
 
 
 def rotation_tables(rows):
@@ -38,97 +42,209 @@
     return x * cosine + swapped * sine
 
 
+def block(i, width=LANES):
+    return pl.ds(pl.multiple_of(i * width, width), width)
+
+
 def split_tp(nx):
     tp = lax.axis_index("tp")
     return tp // nx, tp % nx
 
 
 class Projection:
-    def __init__(self, ny, nx, rows, w_hbm, wb, hx, pr, rr, sems):
-        self.ny, self.nx, self.rows = ny, nx, rows
+    def __init__(self, grid, axis, w_hbm, wb, hx, pr, rr, sems):
+        self.ny, self.nx = grid
+        self.axis = axis
         self.w, self.wb, self.hx, self.pr, self.rr = w_hbm, wb, hx, pr, rr
         self.w_send, self.w_recv, self.w_local, self.h_send, self.h_recv, self.p_send, self.p_recv = sems
-        self.y, self.x = split_tp(nx)
+        y, x = split_tp(self.nx)
+        self.g, self.o, self.ng, self.no = (y, x, self.ny, self.nx) if axis == "y" else (x, y, self.nx, self.ny)
         self.ep = lax.axis_index("ep")
 
-    def _device(self, y, x):
-        return (self.ep, y * self.nx + x)
-
-    def _weight(self, i):
-        y = lax.rem(self.y + i, self.ny)
-        width = self.nx * LANES
-        cols = pl.ds(pl.multiple_of(y * width, width), width)
-        rows = pl.ds(pl.multiple_of(self.y * LANES, LANES), LANES)
+    @staticmethod
+    def scratch(grid, axis, rows):
+        ng, no = grid if axis == "y" else grid[::-1]
+        dma = pltpu.SemaphoreType.DMA
+        return [
+            pltpu.VMEM((ng * LANES, no * LANES), bf16),
+            pltpu.VMEM((rows, ng * LANES), bf16),
+            pltpu.VMEM((no, rows, LANES), bf16),
+            pltpu.VMEM((no, rows, LANES), bf16),
+            dma((ng, no)),
+            dma((ng, no)),
+            dma((no,)),
+            dma((ng,)),
+            dma((ng,)),
+            dma((no,)),
+            dma((no,)),
+        ]
+
+    def _tp(self, g, o):
+        return g * self.nx + o if self.axis == "y" else o * self.nx + g
+
+    def _weights(self, g):
+        rows = block(self.g)
+        if self.axis == "y":
+            width = self.no * LANES
+            yield 0, self.w.at[:, block(g, width)], self.wb.at[rows, :]
+            return
+        for o in range(self.no):
+            yield o, self.w.at[:, block(self._tp(g, o))], self.wb.at[rows, pl.ds(o * LANES, LANES)]
+
+    def _weights_out(self):
+        for i in range(1, self.ng):
+            g = lax.rem(self.g + i, self.ng)
+            for k, source, target in self._weights(g):
+                yield pltpu.make_async_remote_copy(
+                    src_ref=source,
+                    dst_ref=target,
+                    send_sem=self.w_send.at[i, k],
+                    recv_sem=self.w_recv.at[i, k],
+                    device_id=(self.ep, self._tp(g, self.o)),
+                    device_id_type=MESH,
+                )
+
+    def _weights_own(self):
+        for k, source, target in self._weights(self.g):
+            yield pltpu.make_async_copy(source, target, self.w_local.at[k])
+
+    def start_own_weights(self):
+        for copy in self._weights_own():
+            copy.start()
+
+    def start_weights(self):
+        for copy in self._weights_out():
+            copy.start()
+
+    def _gather(self, i):
+        own = self.hx.at[:, block(self.g)]
         return pltpu.make_async_remote_copy(
-            src_ref=self.w.at[:, cols],
-            dst_ref=self.wb.at[rows, :],
-            send_sem=self.w_send.at[i],
-            recv_sem=self.w_recv.at[i],
-            device_id=self._device(y, self.x),
+            src_ref=own,
+            dst_ref=own,
+            send_sem=self.h_send.at[i],
+            recv_sem=self.h_recv.at[i],
+            device_id=(self.ep, self._tp(lax.rem(self.g + i, self.ng), self.o)),
             device_id_type=MESH,
         )
 
-    def _weight_own(self):
-        width = self.nx * LANES
-        cols = pl.ds(pl.multiple_of(self.y * width, width), width)
-        rows = pl.ds(pl.multiple_of(self.y * LANES, LANES), LANES)
-        return pltpu.make_async_copy(self.w.at[:, cols], self.wb.at[rows, :], self.w_local)
-
-    def start_weights(self):
-        self._weight_own().start()
-        for i in range(1, self.ny):
-            self._weight(i).start()
-
-    def _gather(self, i):
-        y = lax.rem(self.y + i, self.ny)
-        cols = pl.ds(pl.multiple_of(self.y * LANES, LANES), LANES)
-        return pltpu.make_async_remote_copy(
-            src_ref=self.hx.at[:, cols],
-            dst_ref=self.hx.at[:, cols],
-            send_sem=self.h_send.at[i],
-            recv_sem=self.h_recv.at[i],
-            device_id=self._device(y, self.x),
-            device_id_type=MESH,
-        )
-
     def start_gather(self, h):
-        cols = pl.ds(pl.multiple_of(self.y * LANES, LANES), LANES)
-        self.hx[:, cols] = h
-        for i in range(1, self.ny):
+        self.hx[:, block(self.g)] = h
+        for i in range(1, self.ng):
             self._gather(i).start()
 
     def _partial(self, i):
-        x = lax.rem(self.x + i, self.nx)
         return pltpu.make_async_remote_copy(
             src_ref=self.pr.at[i],
             dst_ref=self.rr.at[i],
             send_sem=self.p_send.at[i],
             recv_sem=self.p_recv.at[i],
-            device_id=self._device(self.y, x),
+            device_id=(self.ep, self._tp(self.g, lax.rem(self.o + i, self.no))),
             device_id_type=MESH,
         )
 
+    def wait_weights(self):
+        for copy in self._weights_own():
+            copy.wait()
+        for copy in self._weights_out():
+            copy.wait()
+
     def multiply_and_send(self):
-        self._weight_own().wait()
-        for i in range(1, self.ny):
-            self._weight(i).wait()
-        for i in range(1, self.ny):
+        for i in range(1, self.ng):
             self._gather(i).wait()
         h = self.hx[...]
-        for i in list(range(1, self.nx)) + [0]:
-            x = lax.rem(self.x + i, self.nx)
-            w = self.wb[:, pl.ds(pl.multiple_of(x * LANES, LANES), LANES)]
+        for i in list(range(1, self.no)) + [0]:
+            w = self.wb[:, block(lax.rem(self.o + i, self.no))]
             self.pr[i] = jnp.dot(h, w, preferred_element_type=f32).astype(bf16)
             if i:
                 self._partial(i).start()
 
     def finish(self):
-        for i in range(1, self.nx):
+        for i in range(1, self.no):
             self._partial(i).wait()
         total = self.pr[0].astype(f32)
-        for i in range(1, self.nx):
+        for i in range(1, self.no):
             total = total + self.rr[i].astype(f32)
         return total
+
+
+class Exchange:
+    def __init__(self, axis, size, send_at, recv_at, send, recv):
+        self.axis, self.size = axis, size
+        self.send_at, self.recv_at, self.send, self.recv = send_at, recv_at, send, recv
+        self.me = lax.axis_index(axis)
+
+    def _copy(self, i):
+        to = lax.rem(self.me + i, self.size)
+        return pltpu.make_async_remote_copy(
+            src_ref=self.send_at(to),
+            dst_ref=self.recv_at(self.me),
+            send_sem=self.send.at[i],
+            recv_sem=self.recv.at[i],
+            device_id={self.axis: to},
+            device_id_type=MESH,
+        )
+
+    def start(self):
+        @pl.loop(1, self.size)
+        def _(i):
+            self._copy(i).start()
+
+    def wait(self):
+        @pl.loop(1, self.size)
+        def _(i):
+            self._copy(i).wait()
+
+
+class Routing:
+    def __init__(self, tokens, experts, cap):
+        self.tokens, self.experts, self.cap = tokens, experts, cap
+
+    @staticmethod
+    def _iota(shape, dim):
+        return lax.broadcasted_iota(jnp.int32, shape, dim)
+
+    @staticmethod
+    def _ones(cond):
+        return jnp.where(cond, 1.0, 0.0).astype(bf16)
+
+    def to_slots(self, routes_t):
+        n, e = self.tokens, self.experts
+        expert = self._iota((e, n), 0)
+        member = self._ones(jnp.logical_or(expert == routes_t[0:1, :], expert == routes_t[1:2, :]))
+        earlier = self._ones(self._iota((n, n), 0) < self._iota((n, n), 1))
+        place = jnp.dot(member, earlier, preferred_element_type=f32).astype(bf16)
+        spread = self._ones(self._iota((e * PAD, e), 0) // PAD == self._iota((e * PAD, e), 1))
+        member = jnp.dot(spread, member, preferred_element_type=f32)
+        place = jnp.dot(spread, place, preferred_element_type=f32)
+        here = (self._iota((e * PAD, n), 0) % PAD).astype(f32)
+        return self._ones(jnp.logical_and(member > 0.5, place == here))
+
+    def from_slots(self, routes):
+        n, e = self.tokens, self.experts
+        expert = self._iota((n, e), 1)
+        members = [self._ones(expert == routes[:, k : k + 1]) for k in range(TOP_K)]
+        earlier = self._ones(self._iota((n, n), 1) < self._iota((n, n), 0))
+        place = jnp.dot(earlier, members[0] + members[1], preferred_element_type=f32).astype(bf16)
+        spread = self._ones(self._iota((e, e * PAD), 1) // PAD == self._iota((e, e * PAD), 0))
+        place = jnp.dot(place, spread, preferred_element_type=f32)
+        here = (self._iota((n, e * PAD), 1) % PAD).astype(f32)
+        out = []
+        for member in members:
+            member = jnp.dot(member, spread, preferred_element_type=f32)
+            out.append(self._ones(jnp.logical_and(member > 0.5, place == here)))
+        return out
+
+    def packing(self, transposed):
+        small, large = self.experts * self.cap, self.experts * PAD
+        shape, dims = ((large, small), (1, 0)) if transposed else ((small, large), (0, 1))
+        row, col = self._iota(shape, dims[0]), self._iota(shape, dims[1])
+        return self._ones(jnp.logical_and(row == col // PAD * self.cap + col % PAD, col % PAD < self.cap))
+
+
+def swiglu(x, weights):
+    both = jnp.dot(x, weights, preferred_element_type=f32)
+    gate, up = both[:, :LANES], both[:, LANES:]
+    return (gate / (1.0 + jnp.exp(-gate)) * up).astype(bf16)
 
 
 class Ring:
@@ -326,37 +442,84 @@
         return (diff * lax.rsqrt(mean + norm_eps) * gain).astype(bf16)
 
 
-def attention_kernel(
-    dims,
-    q_ref, k_ref, v_ref, cos_ref, sin_ref, lam_ref, gain_ref, w_hbm,
-    out_ref,
-    kbuf, vbuf, qz, top, total, acc, wb, hx, pr, rr,
-    ring_recv, ring_send, pass_send, *proj_sems,
-):
-    nz, ny, nx, rows, tile = dims
-    ep = lax.axis_index("ep")
+def kernel(dims, *refs):
+    nz, ny, nx, rows, tile, tokens, experts, cap = dims
+    refs = list(refs)
+
+    def take(n):
+        out = refs[:n]
+        del refs[:n]
+        return out
+
+    q_ref, k_ref, v_ref, cos_ref, sin_ref, lam_ref, gain_ref, wo_hbm = take(8)
+    x_ref, fgain_ref, routes_ref, routes_t_ref, rweight_ref = take(5)
+    wg_hbm, wu_hbm, wd_hbm, sg_hbm, su_hbm, sd_hbm = take(6)
+    attn_ref, moe_ref = take(2)
+    kbuf, vbuf, qz, top, total, acc, ring_recv, ring_send, pass_send = take(9)
+    xn, wgu, sgu, w_sem = take(4)
+    out_slots, in_slots, xg, back_out, back_in = take(5)
+    a_send, a_recv, g_send, g_recv, b_send, b_recv = take(6)
+    grid = (ny, nx)
+    ep, tp = lax.axis_index("ep"), lax.axis_index("tp")
+    eps, tps = nz * CORES, ny * nx
+
     ring = Ring(nz, kbuf, vbuf, ring_recv, ring_send, pass_send)
-    proj = Projection(ny, nx, rows, w_hbm, wb, hx, pr, rr, proj_sems)
     soft = Softmax(rows, tile, qz, kbuf, vbuf, top, total, acc)
+    projections = []
+    for axis, weight in zip(AXES, (wo_hbm, wd_hbm, sd_hbm)):
+        wb, hx, pr, rr = take(4)
+        projections.append(Projection(grid, axis, weight, wb, hx, pr, rr, take(7)))
+    out_proj, down, shared_down = projections
+    routing = Routing(tokens, experts, cap)
 
     barrier = pltpu.get_barrier_semaphore()
-    peers = ring.neighbours()
-    peers += [proj._device(lax.rem(proj.y + i, ny), proj.x) for i in range(1, ny)]
-    peers += [proj._device(proj.y, lax.rem(proj.x + i, nx)) for i in range(1, nx)]
-    for peer in peers:
-        pl.semaphore_signal(barrier, inc=1, device_id=peer, device_id_type=MESH)
+    for axis, me, size in (("ep", ep, eps), ("tp", tp, tps)):
+
+        @pl.loop(1, size)
+        def _(i):
+            to = lax.rem(me + i, size)
+            pl.semaphore_signal(barrier, inc=1, device_id={axis: to}, device_id_type=MESH)
+
+    loads = [
+        pltpu.make_async_copy(source, buf.at[:, pl.ds(k * LANES, LANES)], w_sem.at[i])
+        for i, (source, buf, k) in enumerate(
+            ((sg_hbm, sgu, 0), (su_hbm, sgu, 1), (wg_hbm, wgu, 0), (wu_hbm, wgu, 1))
+        )
+    ]
+    for load in loads:
+        load.start()
+    for projection in projections:
+        projection.start_own_weights()
 
     cosine, sine = cos_ref[...], sin_ref[...]
     kbuf[ep] = rotated(k_ref[...], cosine, sine).astype(bf16)
     vbuf[ep] = v_ref[...]
-    pl.semaphore_wait(barrier, len(peers))
+    x = x_ref[...].astype(f32)
+    inverse = lax.rsqrt(jnp.mean(x * x, axis=1, keepdims=True) + norm_eps)
+    xn[...] = (x * inverse * fgain_ref[...]).astype(bf16)
+    to_slots = routing.to_slots(routes_t_ref[...])
+    sent = jnp.dot(to_slots, xn[:, block(tp)], preferred_element_type=f32).astype(bf16)
+    sent = sent.reshape(experts, PAD, LANES)
+    out_slots[...] = sent
+    in_slots[ep] = out_slots[ep]
+
+    pl.semaphore_wait(barrier, eps + tps - 2)
     ring.start_own()
-    proj.start_weights()
+    there = Exchange("ep", eps, lambda i: out_slots.at[i], lambda i: in_slots.at[i], a_send, a_recv)
+    spread = Exchange("tp", tps, lambda i: xg.at[:, block(tp)], lambda i: xg.at[:, block(i)], g_send, g_recv)
+    back = Exchange("ep", eps, lambda i: back_out.at[i], lambda i: back_in.at[i], b_send, b_recv)
+    there.start()
+    shared_down.start_weights()
+    down.start_weights()
+    out_proj.start_weights()
 
     q = rotated(q_ref[...], cosine, sine).astype(bf16).astype(f32) * 0.125
     lane = lax.broadcasted_iota(jnp.int32, q.shape, 1)
     qz[:rows, :] = jnp.where(lane < 64, q, 0.0).astype(bf16)
     qz[rows:, :] = jnp.where(lane < 64, 0.0, q).astype(bf16)
+    loads[0].wait()
+    loads[1].wait()
+    shared_down.start_gather(swiglu(xn[...], sgu[...]))
     soft.diagonal(ep)
 
     @pl.when(ring.c == 1)
@@ -389,91 +552,49 @@
         ring.serve(t, 1)
         use_down(t - 1)
 
+        @pl.when(t == SPREAD_AT)
+        def _():
+            there.wait()
+            arrived = in_slots[...].reshape(experts * PAD, LANES)
+            arrived = jnp.dot(routing.packing(False), arrived, preferred_element_type=f32)
+            xg[:, block(tp)] = arrived.astype(bf16)
+            spread.start()
+
+        @pl.when(t == SHARED_AT)
+        def _():
+            shared_down.wait_weights()
+            shared_down.multiply_and_send()
+
+        @pl.when(t == EXPERT_AT)
+        def _():
+            loads[2].wait()
+            loads[3].wait()
+            spread.wait()
+            down.start_gather(swiglu(xg[...], wgu[...]))
+
     use_up(ring.up_steps)
     use_down(ring.up_steps)
 
-    proj.start_gather(soft.heads(lam_ref[0], gain_ref[...]))
-    proj.multiply_and_send()
+    out_proj.start_gather(soft.heads(lam_ref[0], gain_ref[...]))
+    down.wait_weights()
+    down.multiply_and_send()
+    out_proj.wait_weights()
+    out_proj.multiply_and_send()
+    y = down.finish().astype(bf16)
+    y = jnp.dot(routing.packing(True), y, preferred_element_type=f32).astype(bf16)
+    back_out[...] = y.reshape(experts, PAD, LANES)
+    back_in[ep] = back_out[ep]
+    back.start()
+    attn_ref[...] = out_proj.finish().astype(bf16)
+    mixed = shared_down.finish()
+    chosen = routing.from_slots(routes_ref[...])
     ring.wait_sends()
-    out_ref[...] = proj.finish().astype(bf16)
-
-
-def attention(nz, ny, nx, query_pairs, key_pairs, value_rows, head_lambda, head_gain, out_weight):
-    rows = query_pairs.shape[0]
-    tile = 256 if (2 * rows) % 256 == 0 else 2 * rows
-    cosine, sine = rotation_tables(rows)
-    vmem = pl.BlockSpec(memory_space=pltpu.VMEM)
-    slots = nz * CORES
-    dma = pltpu.SemaphoreType.DMA
-    return pl.pallas_call(
-        functools.partial(attention_kernel, (nz, ny, nx, rows, tile)),
-        out_shape=jax.ShapeDtypeStruct((rows, LANES), bf16),
-        in_specs=[vmem] * 5
-        + [pl.BlockSpec(memory_space=pltpu.SMEM), vmem, pl.BlockSpec(memory_space=pl.ANY)],
-        out_specs=vmem,
-        scratch_shapes=[
-            pltpu.VMEM((slots, rows, LANES), bf16),
-            pltpu.VMEM((slots, rows, LANES), bf16),
-            pltpu.VMEM((2 * rows, LANES), bf16),
-            pltpu.VMEM((2 * rows, LANES), f32),
-            pltpu.VMEM((2 * rows, LANES), f32),
-            pltpu.VMEM((2 * rows, LANES), f32),
-            pltpu.VMEM((ny * LANES, nx * LANES), bf16),
-            pltpu.VMEM((rows, ny * LANES), bf16),
-            pltpu.VMEM((nx, rows, LANES), bf16),
-            pltpu.VMEM((nx, rows, LANES), bf16),
-            dma((slots, 2)),
-            dma((nz + 1, 2)),
-            dma((nz, 2)),
-            dma((ny,)),
-            dma((ny,)),
-            dma(()),
-            dma((ny,)),
-            dma((ny,)),
-            dma((nx,)),
-            dma((nx,)),
-        ],
-        compiler_params=pltpu.CompilerParams(
-            collective_id=0, has_side_effects=True, vmem_limit_bytes=56 * 1024 * 1024
-        ),
-        name="attention",
-    )(query_pairs, key_pairs, value_rows, cosine, sine, head_lambda, head_gain.reshape(1, -1), out_weight)
-
-
-def in_blocks(x, dim, peers):
-    shape = x.shape
-    pieces = x.reshape(*shape[:dim], peers, shape[dim] // peers, *shape[dim + 1 :])
-    return jnp.moveaxis(pieces, dim, 0)
-
-
-def sum_at_owner(x, axis, dim):
-    peers = lax.axis_size(axis)
-    pieces = lax.all_to_all(in_blocks(x, dim, peers), axis, 0, 0, tiled=True)
-    return jnp.sum(pieces.astype(jnp.float32), axis=0)
-
-
-def joined_along(pieces, dim):
-    shape = list(pieces.shape[1:])
-    shape[dim] *= pieces.shape[0]
-    return jnp.moveaxis(pieces, 0, dim).reshape(shape)
-
-
-def copy_for_each(x, axis):
-    copies = jnp.broadcast_to(x, (lax.axis_size(axis), *x.shape))
-    return lax.all_to_all(copies, axis, split_axis=0, concat_axis=0, tiled=True)
-
-
-def gather_directly(x, axis, dim):
-    return joined_along(copy_for_each(x, axis), dim)
-
-
-def sent_together(arrays, axis, dim, along):
-    both = jnp.concatenate(arrays, axis=along)
-    out, at, finished = (sum_at_owner(both, axis, dim), 0, [])
-    for a in arrays:
-        finished.append(lax.slice_in_dim(out, at, at + a.shape[along], axis=along))
-        at += a.shape[along]
-    return tuple(finished)
+    back.wait()
+    returned = back_in[...].reshape(experts * PAD, LANES)
+    picked = [jnp.dot(c, returned, preferred_element_type=f32) for c in chosen]
+    weight = rweight_ref[...]
+    mixed = weight[:, 0:1] * picked[0] + weight[:, 1:2] * picked[1] + mixed
+    moe_ref[...] = mixed.astype(bf16)
 
 
 def local(
@@ -495,50 +616,82 @@
     shared_up,
     shared_down,
 ):
-    attn_out = attention(*sizes, query_pairs, key_pairs, value_rows, head_lambda, head_gain, out_weight)
-    row_values = moe_input.astype(jnp.float32)
-    inverse_norm = lax.rsqrt(jnp.mean(row_values * row_values, axis=-1, keepdims=True) + norm_eps)
-    normed = (row_values * inverse_norm * ffn_gain).astype(jnp.bfloat16)
-    token_rows = normed.shape[0]
-    experts = lax.axis_size("ep")
-    capacity = token_rows * TOP_K * 6 // (5 * experts)
-    flat_routes = routes.reshape(-1)
-    onehot = (flat_routes[:, None] == jnp.arange(experts, dtype=jnp.int32)).astype(jnp.int32)
-    slot_rank = jnp.sum((jnp.cumsum(onehot, axis=0) - 1) * onehot, axis=-1)
-    slot_index = flat_routes * capacity + slot_rank
-    token_index = jnp.arange(token_rows * TOP_K, dtype=jnp.int32) // TOP_K
-    slot_rows = (
-        jnp.full((experts * capacity,), token_rows, jnp.int32).at[slot_index].set(token_index)
+    nz, ny, nx = sizes
+    grid = (ny, nx)
+    rows, tokens, width = query_pairs.shape[0], moe_input.shape[0], moe_input.shape[1]
+    slots, experts = nz * CORES, nz * CORES
+    cap = 12
+    tile = 256 if (2 * rows) % 256 == 0 else 2 * rows
+    cosine, sine = rotation_tables(rows)
+    vmem, hbm = pl.BlockSpec(memory_space=pltpu.VMEM), pl.BlockSpec(memory_space=pl.ANY)
+    dma = pltpu.SemaphoreType.DMA
+    scratch = [
+        pltpu.VMEM((slots, rows, LANES), bf16),
+        pltpu.VMEM((slots, rows, LANES), bf16),
+        pltpu.VMEM((2 * rows, LANES), bf16),
+        pltpu.VMEM((2 * rows, LANES), f32),
+        pltpu.VMEM((2 * rows, LANES), f32),
+        pltpu.VMEM((2 * rows, LANES), f32),
+        dma((slots, 2)),
+        dma((nz + 1, 2)),
+        dma((nz, 2)),
+        pltpu.VMEM((tokens, width), bf16),
+        pltpu.VMEM((width, 2 * LANES), bf16),
+        pltpu.VMEM((width, 2 * LANES), bf16),
+        dma((4,)),
+        pltpu.VMEM((experts, PAD, LANES), bf16),
+        pltpu.VMEM((experts, PAD, LANES), bf16),
+        pltpu.VMEM((experts * cap, width), bf16),
+        pltpu.VMEM((experts, PAD, LANES), bf16),
+        pltpu.VMEM((experts, PAD, LANES), bf16),
+        dma((slots,)),
+        dma((slots,)),
+        dma((ny * nx,)),
+        dma((ny * nx,)),
+        dma((slots,)),
+        dma((slots,)),
+    ]
+    for axis, height in zip(AXES, (rows, experts * cap, tokens)):
+        scratch += Projection.scratch(grid, axis, height)
+    return tuple(
+        pl.pallas_call(
+            functools.partial(kernel, (nz, ny, nx, rows, tile, tokens, experts, cap)),
+            out_shape=[
+                jax.ShapeDtypeStruct((rows, LANES), bf16),
+                jax.ShapeDtypeStruct((tokens, LANES), bf16),
+            ],
+            in_specs=[vmem] * 5
+            + [pl.BlockSpec(memory_space=pltpu.SMEM), vmem, hbm]
+            + [vmem] * 5
+            + [hbm] * 6,
+            out_specs=[vmem, vmem],
+            scratch_shapes=scratch,
+            compiler_params=pltpu.CompilerParams(
+                collective_id=0, has_side_effects=True, vmem_limit_bytes=56 * 1024 * 1024
+            ),
+            name="layer",
+        )(
+            query_pairs,
+            key_pairs,
+            value_rows,
+            cosine,
+            sine,
+            head_lambda,
+            head_gain.reshape(1, -1),
+            out_weight,
+            moe_input,
+            ffn_gain.reshape(1, -1),
+            routes,
+            routes.T,
+            route_weight,
+            gate_weight[0],
+            up_weight[0],
+            down_weight[0],
+            shared_gate,
+            shared_up,
+            shared_down,
+        )
     )
-    padded = jnp.concatenate([normed, jnp.zeros((1, normed.shape[1]), jnp.bfloat16)], axis=0)
-    column_width = normed.shape[1] // lax.axis_size("tp")
-    padded_cols = lax.dynamic_slice_in_dim(
-        padded, lax.axis_index("tp") * column_width, column_width, 1
-    )
-    outgoing = padded_cols[slot_rows]
-    arrived = lax.all_to_all(outgoing, "ep", split_axis=0, concat_axis=0, tiled=True)
-    pieces = gather_directly(arrived, "tp", 1)
-    gate_rows = gate_weight[0]
-    up_rows = up_weight[0]
-    gate_part = jnp.dot(pieces, gate_rows, preferred_element_type=jnp.float32)
-    up_part = jnp.dot(pieces, up_rows, preferred_element_type=jnp.float32)
-    hidden = (jax.nn.silu(gate_part) * up_part).astype(jnp.bfloat16)
-    expert_terms = jnp.dot(hidden, down_weight[0], preferred_element_type=jnp.float32)
-    shared_gated = jnp.dot(normed, shared_gate, preferred_element_type=jnp.float32)
-    shared_lifted = jnp.dot(normed, shared_up, preferred_element_type=jnp.float32)
-    shared_hidden = (jax.nn.silu(shared_gated) * shared_lifted).astype(jnp.bfloat16)
-    shared_terms = jnp.dot(shared_hidden, shared_down, preferred_element_type=jnp.float32)
-    expert_sum, shared_sum = sent_together(
-        (expert_terms.astype(jnp.bfloat16), shared_terms.astype(jnp.bfloat16)), "tp", 1, 0
-    )
-    returned = lax.all_to_all(
-        expert_sum.astype(jnp.bfloat16), "ep", split_axis=0, concat_axis=0, tiled=True
-    )
-    picked = returned[slot_index.reshape(token_rows, TOP_K)]
-    moe_out = (
-        jnp.sum(route_weight[..., None] * picked.astype(jnp.float32), axis=1) + shared_sum
-    ).astype(jnp.bfloat16)
-    return (attn_out, moe_out)
 
 
 def grid_of(mesh):

time: 192 us -> 101 us (0.53)
  the two profiles are of different devices: /device:TPU:384 before, /device:TPU:1 now
where the time goes in v2:
time: 101 us
  Pallas kernels  93.7 us (93%)
  local copies, waits for them, and re-layouts  4.34 us (4%)
  other arithmetic  1.53 us (2%)
  between operations  1.34 us (1%)
    pallas_call x1, Pallas kernels, local(): pl.pallas_call(functools.partial(kernel, (nz, ny, nx, rows, tile, tokens,...  93.7 us
    unnamed x10, local copies, waits for them, and re-layouts  4.34 us

profile of v2, /device:TPU:1, one launch (start us, length us, event | category | flops | bytes accessed | tf_op | source)
XLA Modules:
  0.0 101.0 jit_solution(1482885031942524181)
XLA Ops:
  1.3 0.0 copy-start.2
  1.3 0.7 copy-done.2
  2.0 0.0 copy-start.1
  2.0 0.7 copy.19.refs_12_
  2.7 0.0 copy-done.1
  2.8 0.8 copy.18.refs_10_
  3.5 1.5 %select_multiply_fusion = (f32[384,128]{1,0:T(8,128)}, f32[384,128]{1,0:T(8,128)}) fusion(s32[128]{0:T(128)S(1)} %get-tuple-element.6, s32[128]{0:T(128)S(1)} %get-tuple-element.8, s32[128]{0:T(128)S(1)} %get-tuple-element.7, s32[128]{0:T(128)S(1)} %get-tuple-element.9, f32[384]{0:T(512)S(1)} %add_convert_fusion, pred[128]{0:T(512)(128)(4,1)S(1)} %get-tuple-element.4, ...), kind=kLoop, calls=%fused_computation | loop fusion | flops 491520 | bytes 397056 | tf_op jit(solution)/shard_map/mul | solution.py:35
  5.0 93.7 %layer.1 = (bf16[384,128]{1,0:T(8,128)(2,1)}, bf16[160,128]{1,0:T(8,128)(2,1)}) custom-call(bf16[384,128]{1,0:T(8,128)(2,1)} %refs_0_.1, bf16[384,128]{1,0:T(8,128)(2,1)} %refs_1_.1, bf16[384,128]{1,0:T(8,128)(2,1)} %refs_2_.1, f32[384,128]{1,0:T(8,128)} %get-tuple-element.3.refs_3_, f32[384,128]{1,0:T(8,128)} %get-tuple-element.2.refs_4_, ...), custom_call_target="tpu_custom_call" | custom-call | tf_op jit(solution)/shard_map/layer/pallas_call | solution.py:657
  98.8 0.0 copy-start
  98.8 1.5 %copy.23 = bf16[384,128]{1,0:T(8,128)(2,1)} copy(bf16[384,128]{1,0:T(8,128)(2,1)} %get-tuple-element.12) | data formatting | bytes 196608
  100.3 0.0 copy-done
  100.3 0.6 copy.24
  (4 shorter events, 0.0 us)
Async XLA Ops:
  1.3 0.7 copy-start.2
  2.0 0.8 copy-start.1
  98.8 1.6 %copy-start = (bf16[160,128]{1,0:T(8,128)(2,1)S(1)}, bf16[160,128]{1,0:T(8,128)(2,1)}, u32[]{:S(2)}) copy-start(bf16[160,128]{1,0:T(8,128)(2,1)} %get-tuple-element.13) | copy-start | bytes 122884

commit v3 on v2

--- a/solution.py
+++ b/solution.py
@@ -20,19 +20,34 @@
 f32 = jnp.float32
 bf16 = jnp.bfloat16
 
-AXES = ("y", "x", "x")
-SPREAD_AT, SHARED_AT, EXPERT_AT = 2, 3, 6
-
-
-def rotation_tables(rows):
-    shape = (rows, LANES)
+AXES = ("x", "x", "y")
+SPREAD_AT, RELAY_AT, SHARED_AT, EXPERT_AT, DOWN_AT, BACK_AT = 1, 2, 3, 5, 6, 8
+
+
+def frequencies():
+    place = (jnp.arange(LANES, dtype=jnp.int32) % 32).astype(f32)
+    return (theta_base ** (-(place * 2.0) / 64)).reshape(1, LANES)
+
+
+def angle_tables(ep, rows, frequency):
+    quarter = rows // 4
+    shape = (quarter, LANES)
     lane = lax.broadcasted_iota(jnp.int32, shape, 1)
-    place = (lane % 32).astype(f32)
-    frequency = theta_base ** (-(place * 2.0) / 64)
-    positions = lax.axis_index("ep") * rows + lax.broadcasted_iota(jnp.int32, shape, 0)
+    group = lane // 32
+    positions = ep * rows + group * quarter + lax.broadcasted_iota(jnp.int32, shape, 0)
     angles = positions.astype(f32) * frequency
     sign = jnp.where(lane % 64 < 32, -1.0, 1.0)
-    return jnp.cos(angles), jnp.sin(angles) * sign
+
+    def spread(table, g):
+        x = jnp.where(group == g, table, 0.0)
+        x = x + pltpu.roll(x, 32, 1)
+        return x + pltpu.roll(x, 64, 1)
+
+    cosine, sine = jnp.cos(angles), jnp.sin(angles)
+    return (
+        jnp.concatenate([spread(cosine, g) for g in range(4)], axis=0),
+        jnp.concatenate([spread(sine, g) * sign for g in range(4)], axis=0),
+    )
 
 
 def rotated(x, cosine, sine):
@@ -51,12 +66,18 @@
     return tp // nx, tp % nx
 
 
+def arrived(ref, sem):
+    pltpu.make_async_copy(ref, ref, sem).wait()
+
+
 class Projection:
     def __init__(self, grid, axis, w_hbm, wb, hx, pr, rr, sems):
         self.ny, self.nx = grid
         self.axis = axis
         self.w, self.wb, self.hx, self.pr, self.rr = w_hbm, wb, hx, pr, rr
-        self.w_send, self.w_recv, self.w_local, self.h_send, self.h_recv, self.p_send, self.p_recv = sems
+        names = ("w_send", "w_recv", "w_local", "h_send", "h_recv", "p_send", "p_recv")
+        for i, name in enumerate(names):
+            setattr(self, name, sems.at[i])
         y, x = split_tp(self.nx)
         self.g, self.o, self.ng, self.no = (y, x, self.ny, self.nx) if axis == "y" else (x, y, self.nx, self.ny)
         self.ep = lax.axis_index("ep")
@@ -70,13 +91,7 @@
             pltpu.VMEM((rows, ng * LANES), bf16),
             pltpu.VMEM((no, rows, LANES), bf16),
             pltpu.VMEM((no, rows, LANES), bf16),
-            dma((ng, no)),
-            dma((ng, no)),
-            dma((no,)),
-            dma((ng,)),
-            dma((ng,)),
-            dma((no,)),
-            dma((no,)),
+            dma((7,)),
         ]
 
     def _tp(self, g, o):
@@ -86,43 +101,41 @@
         rows = block(self.g)
         if self.axis == "y":
             width = self.no * LANES
-            yield 0, self.w.at[:, block(g, width)], self.wb.at[rows, :]
+            yield self.w.at[:, block(g, width)], self.wb.at[rows, :]
             return
         for o in range(self.no):
-            yield o, self.w.at[:, block(self._tp(g, o))], self.wb.at[rows, pl.ds(o * LANES, LANES)]
-
-    def _weights_out(self):
+            yield self.w.at[:, block(self._tp(g, o))], self.wb.at[rows, pl.ds(o * LANES, LANES)]
+
+    def start_own_weights(self):
+        for source, target in self._weights(self.g):
+            pltpu.make_async_copy(source, target, self.w_local).start()
+
+    def start_weights(self):
         for i in range(1, self.ng):
             g = lax.rem(self.g + i, self.ng)
-            for k, source, target in self._weights(g):
-                yield pltpu.make_async_remote_copy(
+            for source, target in self._weights(g):
+                pltpu.make_async_remote_copy(
                     src_ref=source,
                     dst_ref=target,
-                    send_sem=self.w_send.at[i, k],
-                    recv_sem=self.w_recv.at[i, k],
+                    send_sem=self.w_send,
+                    recv_sem=self.w_recv,
                     device_id=(self.ep, self._tp(g, self.o)),
                     device_id_type=MESH,
-                )
-
-    def _weights_own(self):
-        for k, source, target in self._weights(self.g):
-            yield pltpu.make_async_copy(source, target, self.w_local.at[k])
-
-    def start_own_weights(self):
-        for copy in self._weights_own():
-            copy.start()
-
-    def start_weights(self):
-        for copy in self._weights_out():
-            copy.start()
+                ).start()
+
+    def wait_weights(self):
+        one, others = self.wb.at[pl.ds(0, LANES), :], self.wb.at[pl.ds(0, (self.ng - 1) * LANES), :]
+        arrived(one, self.w_local)
+        arrived(others, self.w_recv)
+        arrived(others, self.w_send)
 
     def _gather(self, i):
         own = self.hx.at[:, block(self.g)]
         return pltpu.make_async_remote_copy(
             src_ref=own,
             dst_ref=own,
-            send_sem=self.h_send.at[i],
-            recv_sem=self.h_recv.at[i],
+            send_sem=self.h_send,
+            recv_sem=self.h_recv,
             device_id=(self.ep, self._tp(lax.rem(self.g + i, self.ng), self.o)),
             device_id_type=MESH,
         )
@@ -136,21 +149,16 @@
         return pltpu.make_async_remote_copy(
             src_ref=self.pr.at[i],
             dst_ref=self.rr.at[i],
-            send_sem=self.p_send.at[i],
-            recv_sem=self.p_recv.at[i],
+            send_sem=self.p_send,
+            recv_sem=self.p_recv,
             device_id=(self.ep, self._tp(self.g, lax.rem(self.o + i, self.no))),
             device_id_type=MESH,
         )
 
-    def wait_weights(self):
-        for copy in self._weights_own():
-            copy.wait()
-        for copy in self._weights_out():
-            copy.wait()
-
     def multiply_and_send(self):
-        for i in range(1, self.ng):
-            self._gather(i).wait()
+        others = self.hx.at[:, pl.ds(0, (self.ng - 1) * LANES)]
+        arrived(others, self.h_recv)
+        arrived(others, self.h_send)
         h = self.hx[...]
         for i in list(range(1, self.no)) + [0]:
             w = self.wb[:, block(lax.rem(self.o + i, self.no))]
@@ -159,8 +167,9 @@
                 self._partial(i).start()
 
     def finish(self):
-        for i in range(1, self.no):
-            self._partial(i).wait()
+        others = self.rr.at[pl.ds(1, self.no - 1)]
+        arrived(others, self.p_recv)
+        arrived(others, self.p_send)
         total = self.pr[0].astype(f32)
         for i in range(1, self.no):
             total = total + self.rr[i].astype(f32)
@@ -168,31 +177,77 @@
 
 
 class Exchange:
-    def __init__(self, axis, size, send_at, recv_at, send, recv):
+    def __init__(self, axis, size, send_at, recv_at, others, sems):
         self.axis, self.size = axis, size
-        self.send_at, self.recv_at, self.send, self.recv = send_at, recv_at, send, recv
+        self.send_at, self.recv_at, self.others = send_at, recv_at, others
+        self.send, self.recv = sems.at[0], sems.at[1]
         self.me = lax.axis_index(axis)
-
-    def _copy(self, i):
-        to = lax.rem(self.me + i, self.size)
-        return pltpu.make_async_remote_copy(
-            src_ref=self.send_at(to),
-            dst_ref=self.recv_at(self.me),
-            send_sem=self.send.at[i],
-            recv_sem=self.recv.at[i],
-            device_id={self.axis: to},
-            device_id_type=MESH,
-        )
 
     def start(self):
         @pl.loop(1, self.size)
         def _(i):
-            self._copy(i).start()
+            to = lax.rem(self.me + i, self.size)
+            pltpu.make_async_remote_copy(
+                src_ref=self.send_at(to),
+                dst_ref=self.recv_at(self.me),
+                send_sem=self.send,
+                recv_sem=self.recv,
+                device_id={self.axis: to},
+                device_id_type=MESH,
+            ).start()
 
     def wait(self):
-        @pl.loop(1, self.size)
-        def _(i):
-            self._copy(i).wait()
+        arrived(self.others, self.recv)
+        arrived(self.others, self.send)
+
+
+class Spread:
+    def __init__(self, grid, ref, sems):
+        self.ny, self.nx = grid
+        self.ref, self.sems = ref, sems
+        self.y, self.x = split_tp(self.nx)
+        self.ep, self.tp = lax.axis_index("ep"), lax.axis_index("tp")
+        half = ref.shape[0] // 2
+        self.upper, self.lower = pl.ds(0, half), pl.ds(half, half)
+
+    def _send(self, ref, y, x, stage):
+        pltpu.make_async_remote_copy(
+            src_ref=ref,
+            dst_ref=ref,
+            send_sem=self.sems.at[stage],
+            recv_sem=self.sems.at[4 + stage],
+            device_id=(self.ep, y * self.nx + x),
+            device_id_type=MESH,
+        ).start()
+
+    def _wait(self, rows, blocks, stage):
+        ref = self.ref.at[rows, pl.ds(0, blocks * LANES)]
+        arrived(ref, self.sems.at[4 + stage])
+        return lambda: arrived(ref, self.sems.at[stage])
+
+    def start(self):
+        for i in range(1, self.nx):
+            self._send(self.ref.at[self.upper, block(self.tp)], self.y, lax.rem(self.x + i, self.nx), 0)
+        for i in range(1, self.ny):
+            self._send(self.ref.at[self.lower, block(self.tp)], lax.rem(self.y + i, self.ny), self.x, 1)
+
+    def relay(self):
+        sent = [self._wait(self.upper, self.nx - 1, 0), self._wait(self.lower, self.ny - 1, 1)]
+        for i in range(1, self.ny):
+            ref = self.ref.at[self.upper, block(self.y, self.nx * LANES)]
+            self._send(ref, lax.rem(self.y + i, self.ny), self.x, 2)
+        for i in range(1, self.nx):
+            for y in range(self.ny):
+                ref = self.ref.at[self.lower, block(y * self.nx + self.x)]
+                self._send(ref, self.y, lax.rem(self.x + i, self.nx), 3)
+        for wait in sent:
+            wait()
+
+    def wait(self):
+        blocks = (self.nx - 1) * self.ny
+        sent = [self._wait(self.upper, (self.ny - 1) * self.nx, 2), self._wait(self.lower, blocks, 3)]
+        for wait in sent:
+            wait()
 
 
 class Routing:
@@ -219,10 +274,15 @@
         here = (self._iota((e * PAD, n), 0) % PAD).astype(f32)
         return self._ones(jnp.logical_and(member > 0.5, place == here))
 
-    def from_slots(self, routes):
+    def column(self, row):
+        n = self.tokens
+        same = self._iota((n, n), 0) == self._iota((n, n), 1)
+        return jnp.sum(jnp.where(same, row.astype(f32), 0.0), axis=1, keepdims=True)
+
+    def from_slots(self, routes_t):
         n, e = self.tokens, self.experts
-        expert = self._iota((n, e), 1)
-        members = [self._ones(expert == routes[:, k : k + 1]) for k in range(TOP_K)]
+        expert = self._iota((n, e), 1).astype(f32)
+        members = [self._ones(expert == self.column(routes_t[k : k + 1, :])) for k in range(TOP_K)]
         earlier = self._ones(self._iota((n, n), 1) < self._iota((n, n), 0))
         place = jnp.dot(earlier, members[0] + members[1], preferred_element_type=f32).astype(bf16)
         spread = self._ones(self._iota((e, e * PAD), 1) // PAD == self._iota((e, e * PAD), 0))
@@ -392,18 +452,21 @@
 
 
 class Softmax:
-    def __init__(self, rows, tile, qz, kbuf, vbuf, top, total, acc):
+    def __init__(self, rows, tile, qz, kbuf, vbuf, top, acc, scores):
         self.rows, self.tile = rows, tile
         self.qz, self.kbuf, self.vbuf = qz, kbuf, vbuf
-        self.top, self.total, self.acc = top, total, acc
-
-    def _tiles(self):
-        return [pl.ds(i * self.tile, self.tile) for i in range(2 * self.rows // self.tile)]
+        self.top, self.acc, self.scores = top, acc, scores
+        self.tiles = [pl.ds(i * tile, tile) for i in range(2 * rows // tile)]
+
+    @staticmethod
+    def _summed(p, values):
+        ones = jnp.ones(values.shape, bf16)
+        return jnp.dot(p.astype(bf16), jnp.concatenate([values, ones], axis=1), preferred_element_type=f32)
 
     def diagonal(self, slot):
         keys, values = self.kbuf[slot], self.vbuf[slot]
-        for i, rows in enumerate(self._tiles()):
-            s = lax.dot_general(self.qz[rows, :], keys, (((1,), (1,)), ((), ())), preferred_element_type=f32)
+        for i, rows in enumerate(self.tiles):
+            s = jnp.dot(self.qz[rows, :], keys, preferred_element_type=f32)
             row = i * self.tile + lax.broadcasted_iota(jnp.int32, s.shape, 0)
             row = jnp.where(row >= self.rows, row - self.rows, row)
             allowed = lax.broadcasted_iota(jnp.int32, s.shape, 1) <= row
@@ -411,32 +474,49 @@
             top = jnp.max(s, axis=1, keepdims=True)
             p = jnp.where(allowed, jnp.exp(s - top), 0.0)
             self.top[rows, :] = jnp.broadcast_to(top, (self.tile, LANES))
-            self.total[rows, :] = jnp.broadcast_to(jnp.sum(p, axis=1, keepdims=True), (self.tile, LANES))
-            self.acc[rows, :] = jnp.dot(p.astype(bf16), values, preferred_element_type=f32)
+            self.acc[rows, :] = self._summed(p, values)
 
     def _add(self, keys, values):
-        for rows in self._tiles():
-            s = lax.dot_general(self.qz[rows, :], keys, (((1,), (1,)), ((), ())), preferred_element_type=f32)
+        count = keys.shape[1]
+        cuts = [(j, min(2 * LANES, count - j)) for j in range(0, count, 2 * LANES)]
+        tops = {}
+
+        def score(i, j, width):
+            s = jnp.dot(self.qz[self.tiles[i], :], keys[:, j : j + width], preferred_element_type=f32)
+            self.scores[i % 2, :, j : j + width] = s
+            for k in range(0, width, LANES):
+                part = s[:, k : k + LANES]
+                tops[i] = jnp.maximum(tops[i], part) if i in tops else part
+
+        for j, width in cuts:
+            score(0, j, width)
+        for i, rows in enumerate(self.tiles):
             before = self.top[rows, :]
-            top = jnp.maximum(before, jnp.max(s, axis=1, keepdims=True))
-            p = jnp.exp(s - top[:, :1])
+            top = jnp.maximum(before, jnp.max(tops[i], axis=1, keepdims=True))
             scale = jnp.exp(before - top)
             self.top[rows, :] = top
-            self.total[rows, :] = self.total[rows, :] * scale + jnp.sum(p, axis=1, keepdims=True)
-            self.acc[rows, :] = self.acc[rows, :] * scale + jnp.dot(
-                p.astype(bf16), values, preferred_element_type=f32
-            )
+            total = self.acc[rows, :] * jnp.concatenate([scale, scale], axis=1)
+            for j, width in cuts:
+                if i + 1 < len(self.tiles):
+                    score(i + 1, j, width)
+                s = self.scores[i % 2, :, j : j + width]
+                p = jnp.exp(s - jnp.concatenate([top] * (width // LANES), axis=1))
+                total = total + self._summed(p, values[j : j + width])
+            self.acc[rows, :] = total
 
     def one(self, slot):
         self._add(self.kbuf[slot], self.vbuf[slot])
 
     def chip(self, source):
-        pair = pl.ds(source * CORES, CORES)
-        shape = (CORES * self.rows, LANES)
-        self._add(self.kbuf[pair].reshape(shape), self.vbuf[pair].reshape(shape))
+        first, second = source * CORES, source * CORES + 1
+        self._add(
+            jnp.concatenate([self.kbuf[first], self.kbuf[second]], axis=1),
+            jnp.concatenate([self.vbuf[first], self.vbuf[second]], axis=0),
+        )
 
     def heads(self, lam, gain):
-        out = self.acc[...] / self.total[...]
+        acc = self.acc[...]
+        out = acc[:, :LANES] / acc[:, LANES:]
         diff = out[: self.rows] - lam * out[self.rows :]
         mean = jnp.mean(diff * diff, axis=1, keepdims=True)
         return (diff * lax.rsqrt(mean + norm_eps) * gain).astype(bf16)
@@ -451,24 +531,28 @@
         del refs[:n]
         return out
 
-    q_ref, k_ref, v_ref, cos_ref, sin_ref, lam_ref, gain_ref, wo_hbm = take(8)
-    x_ref, fgain_ref, routes_ref, routes_t_ref, rweight_ref = take(5)
-    wg_hbm, wu_hbm, wd_hbm, sg_hbm, su_hbm, sd_hbm = take(6)
-    attn_ref, moe_ref = take(2)
-    kbuf, vbuf, qz, top, total, acc, ring_recv, ring_send, pass_send = take(9)
-    xn, wgu, sgu, w_sem = take(4)
+    inputs = take(8)
+    (v_hbm,) = take(1)
+    lam_ref, wo_hbm, wg_hbm, wu_hbm, wd_hbm, sg_hbm, su_hbm, sd_hbm = take(8)
+    attn_hbm, moe_hbm = take(2)
+    buffers = take(7)
+    (load_sem,) = take(1)
+    q_ref, k_ref, freq_ref, gain_ref, x_ref, fgain_ref, routes_ref = buffers
+    kbuf, vbuf, qz, top, acc, scores, ring_recv, ring_send, pass_send = take(9)
+    xn, wgu, sgu = take(3)
     out_slots, in_slots, xg, back_out, back_in = take(5)
-    a_send, a_recv, g_send, g_recv, b_send, b_recv = take(6)
+    a_sems, g_sems, b_sems = take(3)
+    attn_ref, moe_ref, rweight_ref, sine_ref, cosine_ref = take(5)
     grid = (ny, nx)
     ep, tp = lax.axis_index("ep"), lax.axis_index("tp")
     eps, tps = nz * CORES, ny * nx
 
     ring = Ring(nz, kbuf, vbuf, ring_recv, ring_send, pass_send)
-    soft = Softmax(rows, tile, qz, kbuf, vbuf, top, total, acc)
+    soft = Softmax(rows, tile, qz, kbuf, vbuf, top, acc, scores)
     projections = []
     for axis, weight in zip(AXES, (wo_hbm, wd_hbm, sd_hbm)):
-        wb, hx, pr, rr = take(4)
-        projections.append(Projection(grid, axis, weight, wb, hx, pr, rr, take(7)))
+        wb, hx, pr, rr, sems = take(5)
+        projections.append(Projection(grid, axis, weight, wb, hx, pr, rr, sems))
     out_proj, down, shared_down = projections
     routing = Routing(tokens, experts, cap)
 
@@ -480,47 +564,65 @@
             to = lax.rem(me + i, size)
             pl.semaphore_signal(barrier, inc=1, device_id={axis: to}, device_id_type=MESH)
 
-    loads = [
-        pltpu.make_async_copy(source, buf.at[:, pl.ds(k * LANES, LANES)], w_sem.at[i])
-        for i, (source, buf, k) in enumerate(
-            ((sg_hbm, sgu, 0), (su_hbm, sgu, 1), (wg_hbm, wgu, 0), (wu_hbm, wgu, 1))
-        )
-    ]
-    for load in loads:
+    pairs = zip(inputs, buffers + [rweight_ref])
+    loads = [pltpu.make_async_copy(a, b, load_sem.at[i]) for i, (a, b) in enumerate(pairs)]
+    q_load, k_load, freq_load, gain_load, x_load, fgain_load, routes_load, rweight_load = loads
+    weights = []
+    for i, (source, buf, k) in enumerate(((sg_hbm, sgu, 0), (su_hbm, sgu, 1), (wg_hbm, wgu, 0), (wu_hbm, wgu, 1))):
+        sem = load_sem.at[len(loads) + i]
+        weights.append(pltpu.make_async_copy(source, buf.at[:, pl.ds(k * LANES, LANES)], sem))
+    v_load = pltpu.make_async_copy(v_hbm, vbuf.at[ep], load_sem.at[len(loads) + 4])
+    for load in (freq_load, k_load, v_load, x_load, fgain_load, routes_load, q_load, gain_load, rweight_load):
+        load.start()
+    for load in weights:
         load.start()
     for projection in projections:
         projection.start_own_weights()
 
-    cosine, sine = cos_ref[...], sin_ref[...]
-    kbuf[ep] = rotated(k_ref[...], cosine, sine).astype(bf16)
-    vbuf[ep] = v_ref[...]
-    x = x_ref[...].astype(f32)
-    inverse = lax.rsqrt(jnp.mean(x * x, axis=1, keepdims=True) + norm_eps)
-    xn[...] = (x * inverse * fgain_ref[...]).astype(bf16)
-    to_slots = routing.to_slots(routes_t_ref[...])
-    sent = jnp.dot(to_slots, xn[:, block(tp)], preferred_element_type=f32).astype(bf16)
-    sent = sent.reshape(experts, PAD, LANES)
-    out_slots[...] = sent
-    in_slots[ep] = out_slots[ep]
-
-    pl.semaphore_wait(barrier, eps + tps - 2)
+    with jax.named_scope("pre_angles"):
+        freq_load.wait()
+        cosine, sine = angle_tables(ep, rows, freq_ref[...])
+        cosine_ref[...] = cosine
+        sine_ref[...] = sine
+    with jax.named_scope("pre_keys"):
+        k_load.wait()
+        kbuf[ep] = jnp.transpose(rotated(k_ref[...], cosine_ref[...], sine_ref[...])).astype(bf16)
+    with jax.named_scope("pre_norm"):
+        x_load.wait()
+        fgain_load.wait()
+        x = x_ref[...].astype(f32)
+        inverse = lax.rsqrt(jnp.mean(x * x, axis=1, keepdims=True) + norm_eps)
+        xn[...] = (x * inverse * fgain_ref[...]).astype(bf16)
+    with jax.named_scope("pre_routes"):
+        routes_load.wait()
+        to_slots = routing.to_slots(routes_ref[...])
+        sent = jnp.dot(to_slots, xn[:, block(tp)], preferred_element_type=f32).astype(bf16)
+        out_slots[...] = sent.reshape(experts, PAD, LANES)
+        in_slots[ep] = out_slots[ep]
+        v_load.wait()
+
+    with jax.named_scope("barrier"):
+        pl.semaphore_wait(barrier, eps + tps - 2)
+    slots = pl.ds(0, eps - 1)
+    there = Exchange("ep", eps, lambda i: out_slots.at[i], lambda i: in_slots.at[i], in_slots.at[slots], a_sems)
+    spread = Spread(grid, xg, g_sems)
+    back = Exchange("ep", eps, lambda i: back_out.at[i], lambda i: back_in.at[i], back_in.at[slots], b_sems)
+    there.start()
     ring.start_own()
-    there = Exchange("ep", eps, lambda i: out_slots.at[i], lambda i: in_slots.at[i], a_send, a_recv)
-    spread = Exchange("tp", tps, lambda i: xg.at[:, block(tp)], lambda i: xg.at[:, block(i)], g_send, g_recv)
-    back = Exchange("ep", eps, lambda i: back_out.at[i], lambda i: back_in.at[i], b_send, b_recv)
-    there.start()
+    down.start_weights()
     shared_down.start_weights()
-    down.start_weights()
     out_proj.start_weights()
 
-    q = rotated(q_ref[...], cosine, sine).astype(bf16).astype(f32) * 0.125
+    q_load.wait()
+    q = rotated(q_ref[...], cosine_ref[...], sine_ref[...]).astype(bf16).astype(f32) * 0.125
     lane = lax.broadcasted_iota(jnp.int32, q.shape, 1)
     qz[:rows, :] = jnp.where(lane < 64, q, 0.0).astype(bf16)
     qz[rows:, :] = jnp.where(lane < 64, 0.0, q).astype(bf16)
-    loads[0].wait()
-    loads[1].wait()
-    shared_down.start_gather(swiglu(xn[...], sgu[...]))
-    soft.diagonal(ep)
+    weights[0].wait()
+    weights[1].wait()
+    with jax.named_scope("shared_diagonal"):
+        shared_down.start_gather(swiglu(xn[...], sgu[...]))
+        soft.diagonal(ep)
 
     @pl.when(ring.c == 1)
     def _():
@@ -536,65 +638,98 @@
 
         @pl.when(jnp.logical_and(here, t >= 1))
         def _():
-            use(source)
+            with jax.named_scope("use_up"):
+                use(source)
 
     def use_down(t):
         source, here = ring.down_source(t)
 
         @pl.when(jnp.logical_and(jnp.logical_and(here, t >= 1), source < ring.z))
         def _():
-            use(source)
+            with jax.named_scope("use_down"):
+                use(source)
 
     @pl.loop(1, ring.up_steps + 1)
     def _(t):
-        ring.serve(t, 0)
+        with jax.named_scope("serve_keys"):
+            ring.serve(t, 0)
         use_up(t - 1)
-        ring.serve(t, 1)
+        with jax.named_scope("serve_values"):
+            ring.serve(t, 1)
         use_down(t - 1)
 
         @pl.when(t == SPREAD_AT)
         def _():
-            there.wait()
-            arrived = in_slots[...].reshape(experts * PAD, LANES)
-            arrived = jnp.dot(routing.packing(False), arrived, preferred_element_type=f32)
-            xg[:, block(tp)] = arrived.astype(bf16)
+            with jax.named_scope("there_wait"):
+                there.wait()
+            rows_in = in_slots[...].reshape(experts * PAD, LANES)
+            rows_in = jnp.dot(routing.packing(False), rows_in, preferred_element_type=f32)
+            xg[:, block(tp)] = rows_in.astype(bf16)
             spread.start()
 
         @pl.when(t == SHARED_AT)
         def _():
-            shared_down.wait_weights()
-            shared_down.multiply_and_send()
+            with jax.named_scope("shared_multiply"):
+                shared_down.wait_weights()
+                shared_down.multiply_and_send()
+
+        @pl.when(t == RELAY_AT)
+        def _():
+            with jax.named_scope("relay"):
+                spread.relay()
 
         @pl.when(t == EXPERT_AT)
         def _():
-            loads[2].wait()
-            loads[3].wait()
-            spread.wait()
-            down.start_gather(swiglu(xg[...], wgu[...]))
+            weights[2].wait()
+            weights[3].wait()
+            with jax.named_scope("spread_wait"):
+                spread.wait()
+            with jax.named_scope("experts"):
+                down.start_gather(swiglu(xg[...], wgu[...]))
+
+        @pl.when(t == DOWN_AT)
+        def _():
+            with jax.named_scope("down_multiply"):
+                down.wait_weights()
+                down.multiply_and_send()
+
+        @pl.when(t == BACK_AT)
+        def _():
+            with jax.named_scope("down_finish"):
+                y = down.finish().astype(bf16)
+            y = jnp.dot(routing.packing(True), y, preferred_element_type=f32).astype(bf16)
+            back_out[...] = y.reshape(experts, PAD, LANES)
+            back_in[ep] = back_out[ep]
+            back.start()
 
     use_up(ring.up_steps)
-    use_down(ring.up_steps)
-
-    out_proj.start_gather(soft.heads(lam_ref[0], gain_ref[...]))
-    down.wait_weights()
-    down.multiply_and_send()
-    out_proj.wait_weights()
-    out_proj.multiply_and_send()
-    y = down.finish().astype(bf16)
-    y = jnp.dot(routing.packing(True), y, preferred_element_type=f32).astype(bf16)
-    back_out[...] = y.reshape(experts, PAD, LANES)
-    back_in[ep] = back_out[ep]
-    back.start()
-    attn_ref[...] = out_proj.finish().astype(bf16)
-    mixed = shared_down.finish()
-    chosen = routing.from_slots(routes_ref[...])
-    ring.wait_sends()
-    back.wait()
+    gain_load.wait()
+    with jax.named_scope("heads"):
+        out_proj.start_gather(soft.heads(lam_ref[0], gain_ref[...]))
+    with jax.named_scope("shared_finish"):
+        mixed = shared_down.finish()
+        chosen = routing.from_slots(routes_ref[...])
+    with jax.named_scope("out_multiply"):
+        out_proj.wait_weights()
+        out_proj.multiply_and_send()
+    rweight_load.wait()
+    with jax.named_scope("back_wait"):
+        back.wait()
     returned = back_in[...].reshape(experts * PAD, LANES)
-    picked = [jnp.dot(c, returned, preferred_element_type=f32) for c in chosen]
-    weight = rweight_ref[...]
-    mixed = weight[:, 0:1] * picked[0] + weight[:, 1:2] * picked[1] + mixed
+    for k in range(TOP_K):
+        picked = jnp.dot(chosen[k], returned, preferred_element_type=f32)
+        mixed = mixed + routing.column(rweight_ref[k : k + 1, :]) * picked
     moe_ref[...] = mixed.astype(bf16)
+    moe_store = pltpu.make_async_copy(moe_ref, moe_hbm, load_sem.at[0])
+    moe_store.start()
+    with jax.named_scope("out_finish"):
+        attn_ref[...] = out_proj.finish().astype(bf16)
+    attn_store = pltpu.make_async_copy(attn_ref, attn_hbm, load_sem.at[1])
+    attn_store.start()
+    with jax.named_scope("wait_sends"):
+        ring.wait_sends()
+    moe_store.wait()
+    attn_store.wait()
 
 
 def local(
@@ -622,34 +757,42 @@
     slots, experts = nz * CORES, nz * CORES
     cap = 12
     tile = 256 if (2 * rows) % 256 == 0 else 2 * rows
-    cosine, sine = rotation_tables(rows)
-    vmem, hbm = pl.BlockSpec(memory_space=pltpu.VMEM), pl.BlockSpec(memory_space=pl.ANY)
+    hbm = pl.BlockSpec(memory_space=pl.ANY)
     dma = pltpu.SemaphoreType.DMA
     scratch = [
-        pltpu.VMEM((slots, rows, LANES), bf16),
+        pltpu.VMEM((rows, LANES), bf16),
+        pltpu.VMEM((rows, LANES), bf16),
+        pltpu.VMEM((1, LANES), f32),
+        pltpu.VMEM((1, LANES), f32),
+        pltpu.VMEM((tokens, width), bf16),
+        pltpu.VMEM((1, width), f32),
+        pltpu.VMEM((TOP_K, tokens), jnp.int32),
+        dma((13,)),
+        pltpu.VMEM((slots, LANES, rows), bf16),
         pltpu.VMEM((slots, rows, LANES), bf16),
         pltpu.VMEM((2 * rows, LANES), bf16),
         pltpu.VMEM((2 * rows, LANES), f32),
-        pltpu.VMEM((2 * rows, LANES), f32),
-        pltpu.VMEM((2 * rows, LANES), f32),
+        pltpu.VMEM((2 * rows, 2 * LANES), f32),
+        pltpu.VMEM((2, tile, CORES * rows), f32),
         dma((slots, 2)),
         dma((nz + 1, 2)),
         dma((nz, 2)),
         pltpu.VMEM((tokens, width), bf16),
         pltpu.VMEM((width, 2 * LANES), bf16),
         pltpu.VMEM((width, 2 * LANES), bf16),
-        dma((4,)),
         pltpu.VMEM((experts, PAD, LANES), bf16),
         pltpu.VMEM((experts, PAD, LANES), bf16),
         pltpu.VMEM((experts * cap, width), bf16),
         pltpu.VMEM((experts, PAD, LANES), bf16),
         pltpu.VMEM((experts, PAD, LANES), bf16),
-        dma((slots,)),
-        dma((slots,)),
-        dma((ny * nx,)),
-        dma((ny * nx,)),
-        dma((slots,)),
-        dma((slots,)),
+        dma((2,)),
+        dma((8,)),
+        dma((2,)),
+        pltpu.VMEM((rows, LANES), bf16),
+        pltpu.VMEM((tokens, LANES), bf16),
+        pltpu.VMEM((TOP_K, tokens), f32),
+        pltpu.VMEM((rows, LANES), f32),
+        pltpu.VMEM((rows, LANES), f32),
     ]
     for axis, height in zip(AXES, (rows, experts * cap, tokens)):
         scratch += Projection.scratch(grid, axis, height)
@@ -660,11 +803,8 @@
                 jax.ShapeDtypeStruct((rows, LANES), bf16),
                 jax.ShapeDtypeStruct((tokens, LANES), bf16),
             ],
-            in_specs=[vmem] * 5
-            + [pl.BlockSpec(memory_space=pltpu.SMEM), vmem, hbm]
-            + [vmem] * 5
-            + [hbm] * 6,
-            out_specs=[vmem, vmem],
+            in_specs=[hbm] * 9 + [pl.BlockSpec(memory_space=pltpu.SMEM)] + [hbm] * 7,
+            out_specs=[hbm, hbm],
             scratch_shapes=scratch,
             compiler_params=pltpu.CompilerParams(
                 collective_id=0, has_side_effects=True, vmem_limit_bytes=56 * 1024 * 1024
@@ -673,17 +813,15 @@
         )(
             query_pairs,
             key_pairs,
-            value_rows,
-            cosine,
-            sine,
-            head_lambda,
+            frequencies(),
             head_gain.reshape(1, -1),
-            out_weight,
             moe_input,
             ffn_gain.reshape(1, -1),
-            routes,
             routes.T,
-            route_weight,
+            route_weight.T,
+            value_rows,
+            head_lambda,
+            out_weight,
             gate_weight[0],
             up_weight[0],
             down_weight[0],

time: 101 us -> 78.6 us (0.78)
  the two profiles are of different devices: /device:TPU:1 before, /device:TPU:256 now
where the time goes in v3:
time: 78.6 us; the launch traced here: 78.5 us
  Pallas kernels  74.5 us (95%)
  local copies, waits for them, and re-layouts  2.17 us (3%)
  between operations  1.29 us (2%)
    pallas_call x1, Pallas kernels, local(): pl.pallas_call(functools.partial(kernel, (nz, ny, nx, rows, tile, tokens,...  74.5 us
    unnamed x4, local copies, waits for them, and re-layouts  2.17 us

profile of v3, /device:TPU:256, one launch (start us, length us, event | category | flops | bytes accessed | tf_op | source)
XLA Modules:
  0.0 78.5 jit_solution(12551317912858754508)
XLA Ops:
  1.3 0.5 fusion.4.refs_2_
  1.8 74.5 %layer.1 = (bf16[384,128]{1,0:T(8,128)(2,1)}, bf16[160,128]{1,0:T(8,128)(2,1)}) custom-call(bf16[384,128]{1,0:T(8,128)(2,1)} %refs_0_.1, bf16[384,128]{1,0:T(8,128)(2,1)} %refs_1_.1, f32[1,128]{1,0:T(1,128)} %fusion.4.refs_2_, f32[1,128]{1,0:T(1,128)} %bitcast.13, bf16[160,2048]{1,0:T(8,128)(2,1)} %refs_4_.1, f32[1,2048]{1,0:T(1,128)} %bitcast.10, ...), custom_call_target="tpu_custom_call" | custom-call | tf_op jit(solution)/shard_map/layer/pallas_call | solution.py:800
  76.3 0.0 copy-start
  76.3 1.5 %copy.21 = bf16[384,128]{1,0:T(8,128)(2,1)} copy(bf16[384,128]{1,0:T(8,128)(2,1)} %get-tuple-element.4) | data formatting | bytes 196608
  77.8 0.0 copy-done
  77.8 0.6 copy.22
Async XLA Ops:
  76.3 1.6 %copy-start = (bf16[160,128]{1,0:T(8,128)(2,1)S(1)}, bf16[160,128]{1,0:T(8,128)(2,1)}, u32[]{:S(2)}) copy-start(bf16[160,128]{1,0:T(8,128)(2,1)} %get-tuple-element.5) | copy-start | bytes 122884

commit v4 on v3

--- a/solution.py
+++ b/solution.py
@@ -2,6 +2,7 @@
 
 import jax
 import jax.numpy as jnp
+import numpy as np
 from jax import lax
 from jax.experimental import pallas as pl
 from jax.experimental.pallas import tpu as pltpu
@@ -16,17 +17,18 @@
 CORES = 2
 LANES = 128
 PAD = 16
+PARTS = 4
 MESH = pl.DeviceIdType.MESH
 f32 = jnp.float32
 bf16 = jnp.bfloat16
 
-AXES = ("x", "x", "y")
-SPREAD_AT, RELAY_AT, SHARED_AT, EXPERT_AT, DOWN_AT, BACK_AT = 1, 2, 3, 5, 6, 8
+AXES = ("x", "y", "x", "y")
+RELAY_AT, SHARED_AT, EXPERT_AT, DOWN_AT, BACK_AT = 1, 3, 4, 6, 8
 
 
 def frequencies():
-    place = (jnp.arange(LANES, dtype=jnp.int32) % 32).astype(f32)
-    return (theta_base ** (-(place * 2.0) / 64)).reshape(1, LANES)
+    place = (np.arange(LANES) % 32).astype(np.float32)
+    return np.power(np.float32(theta_base), -(place * np.float32(2.0)) / np.float32(64)).reshape(1, LANES)
 
 
 def angle_tables(ep, rows, frequency):
@@ -184,9 +186,12 @@
         self.me = lax.axis_index(axis)
 
     def start(self):
+        middle = self.size // 2
+
         @pl.loop(1, self.size)
         def _(i):
-            to = lax.rem(self.me + i, self.size)
+            away = jnp.where(i % 2 == 0, middle - i // 2, middle + i // 2)
+            to = lax.rem(self.me + away, self.size)
             pltpu.make_async_remote_copy(
                 src_ref=self.send_at(to),
                 dst_ref=self.recv_at(self.me),
@@ -308,11 +313,12 @@
 
 
 class Ring:
-    def __init__(self, nz, kbuf, vbuf, recv, send, pass_send):
+    def __init__(self, nz, kbuf, vbuf, recv, handed_recv, up_send, down_send, pass_send):
         self.nz = nz
         self.up_steps, self.down_steps = nz // 2, nz - 1 - nz // 2
-        self.bufs = (kbuf, vbuf)
-        self.recv, self.send, self.pass_send = recv, send, pass_send
+        self.kbuf, self.vbuf = kbuf, vbuf
+        self.recv, self.handed_recv = recv, handed_recv
+        self.up_send, self.down_send, self.pass_send = up_send, down_send, pass_send
         ep = lax.axis_index("ep")
         self.tp = lax.axis_index("tp")
         self.z, self.c = ep // CORES, ep % CORES
@@ -320,41 +326,48 @@
     def _device(self, z, c):
         return (z * CORES + c, self.tp)
 
-    def neighbours(self):
-        up = lax.rem(self.z + 1, self.nz)
-        down = lax.rem(self.z + self.nz - 1, self.nz)
-        return [self._device(up, self.c), self._device(down, self.c), self._device(self.z, 1 - self.c)]
-
-    def copy(self, source, part, to_z, sem):
-        slot = source * CORES + self.c
-        ref = self.bufs[part].at[slot]
+    def _piece(self, slot, part):
+        buf = self.kbuf if part < 2 else self.vbuf
+        half = buf.shape[1] // 2
+        return buf.at[slot, pl.ds(part % 2 * half, half)]
+
+    def _copy(self, source, part, to_z, sems):
+        ref = self._piece(source * CORES + self.c, part)
         return pltpu.make_async_remote_copy(
             src_ref=ref,
             dst_ref=ref,
-            send_sem=self.send.at[sem, part],
-            recv_sem=self.recv.at[slot, part],
+            send_sem=sems.at[part],
+            recv_sem=self.recv.at[source, part],
             device_id=self._device(to_z, self.c),
             device_id_type=MESH,
         )
 
     def up(self, source, part):
-        return self.copy(source, part, lax.rem(self.z + 1, self.nz), source)
-
-    def down(self, source, part, sem=None):
-        to = lax.rem(self.z + self.nz - 1, self.nz)
-        return self.copy(source, part, to, source if sem is None else sem)
-
-    def handed(self, source, part, core):
-        slot = source * CORES + core
-        ref = self.bufs[part].at[slot]
-        return pltpu.make_async_remote_copy(
-            src_ref=ref,
-            dst_ref=ref,
-            send_sem=self.pass_send.at[source, part],
-            recv_sem=self.recv.at[slot, part],
-            device_id=self._device(self.z, 1 - self.c),
-            device_id_type=MESH,
-        )
+        return self._copy(source, part, lax.rem(self.z + 1, self.nz), self.up_send)
+
+    def down(self, source, part):
+        return self._copy(source, part, lax.rem(self.z + self.nz - 1, self.nz), self.down_send)
+
+    def _hand(self, source, way):
+        for buf in (self.kbuf, self.vbuf):
+            ref = buf.at[source * CORES + self.c]
+            pltpu.make_async_remote_copy(
+                src_ref=ref,
+                dst_ref=ref,
+                send_sem=self.pass_send.at[way],
+                recv_sem=self.handed_recv.at[source],
+                device_id=self._device(self.z, 1 - self.c),
+                device_id_type=MESH,
+            ).start()
+
+    def _both(self, source):
+        return self.kbuf.at[pl.ds(source * CORES, CORES)]
+
+    def wait_handed(self, source):
+        arrived(self._both(source), self.handed_recv.at[source])
+
+    def _wait_hand_sent(self, way):
+        arrived(self._both(0), self.pass_send.at[way])
 
     def up_source(self, t):
         return self.z - t, self.z - t >= 0
@@ -363,8 +376,12 @@
         source = lax.rem(self.z + t, self.nz)
         return source, jnp.logical_and(source < self.down_steps, t <= self.down_steps)
 
+    def down_used(self, t):
+        source, here = self.down_source(t)
+        return source, jnp.logical_and(here, source < self.z)
+
     def start_own(self):
-        for part in range(2):
+        for part in range(PARTS):
 
             @pl.when(self.z < self.nz - 1)
             def _():
@@ -372,11 +389,11 @@
 
             @pl.when(self.z < self.down_steps)
             def _():
-                self.down(self.z, part, self.nz).start()
-
-            @pl.when(self.c == 0)
-            def _():
-                self.handed(self.z, part, self.c).start()
+                self.down(self.z, part).start()
+
+        @pl.when(self.c == 0)
+        def _():
+            self._hand(self.z, 0)
 
     def serve(self, t, part):
         source, here = self.up_source(t)
@@ -387,11 +404,11 @@
 
             @pl.when(jnp.logical_and(t < self.up_steps, self.z < self.nz - 1))
             def _():
+                self.up(source, part).wait_send()
                 self.up(source, part).start()
 
-            self.handed(source, part, self.c).start()
-
         source_d, here_d = self.down_source(t)
+        _, sent_before = self.down_source(t - 1)
 
         @pl.when(here_d)
         def _():
@@ -399,56 +416,54 @@
 
             @pl.when(t < self.down_steps)
             def _():
+                @pl.when(sent_before)
+                def _():
+                    self.down(source_d, part).wait_send()
+
                 self.down(source_d, part).start()
 
-            @pl.when(source_d < self.z)
+    def hand(self, t):
+        source, here = self.up_source(t)
+
+        @pl.when(here)
+        def _():
+            @pl.when(jnp.logical_or(t > 1, self.c == 0))
             def _():
-                self.handed(source_d, part, self.c).start()
-
-    def wait_handed(self, source):
-        for part in range(2):
-            self.handed(source, part, 1 - self.c).wait_recv()
+                self._wait_hand_sent(0)
+
+            self._hand(source, 0)
+
+        source_d, used = self.down_used(t)
+        _, used_before = self.down_used(t - 1)
+
+        @pl.when(used)
+        def _():
+            @pl.when(used_before)
+            def _():
+                self._wait_hand_sent(1)
+
+            self._hand(source_d, 1)
 
     def wait_sends(self):
-        for part in range(2):
-
-            @pl.when(self.z < self.nz - 1)
-            def _():
+        first_down = self.nz - self.down_steps
+
+        @pl.when(self.z < self.nz - 1)
+        def _():
+            for part in range(PARTS):
                 self.up(self.z, part).wait_send()
 
-            @pl.when(self.z < self.down_steps)
-            def _():
-                self.down(self.z, part, self.nz).wait_send()
-
-            @pl.when(self.c == 0)
-            def _():
-                self.handed(self.z, part, self.c).wait_send()
-
-        @pl.loop(1, self.up_steps + 1)
-        def _(t):
-            source, here = self.up_source(t)
-            source_d, here_d = self.down_source(t)
-
-            @pl.when(here)
-            def _():
-                for part in range(2):
-                    self.handed(source, part, self.c).wait_send()
-
-                    @pl.when(jnp.logical_and(t < self.up_steps, self.z < self.nz - 1))
-                    def _():
-                        self.up(source, part).wait_send()
-
-            @pl.when(here_d)
-            def _():
-                for part in range(2):
-
-                    @pl.when(t < self.down_steps)
-                    def _():
-                        self.down(source_d, part).wait_send()
-
-                    @pl.when(source_d < self.z)
-                    def _():
-                        self.handed(source_d, part, self.c).wait_send()
+        @pl.when(jnp.logical_or(self.z < self.down_steps, self.z > first_down))
+        def _():
+            for part in range(PARTS):
+                self.down(self.z, part).wait_send()
+
+        @pl.when(jnp.logical_or(self.c == 0, self.z >= 1))
+        def _():
+            self._wait_hand_sent(0)
+
+        @pl.when(self.z >= first_down)
+        def _():
+            self._wait_hand_sent(1)
 
 
 class Softmax:
@@ -538,7 +553,8 @@
     buffers = take(7)
     (load_sem,) = take(1)
     q_ref, k_ref, freq_ref, gain_ref, x_ref, fgain_ref, routes_ref = buffers
-    kbuf, vbuf, qz, top, acc, scores, ring_recv, ring_send, pass_send = take(9)
+    kbuf, vbuf, qz, top, acc, scores = take(6)
+    ring_sems = take(5)
     xn, wgu, sgu = take(3)
     out_slots, in_slots, xg, back_out, back_in = take(5)
     a_sems, g_sems, b_sems = take(3)
@@ -547,13 +563,14 @@
     ep, tp = lax.axis_index("ep"), lax.axis_index("tp")
     eps, tps = nz * CORES, ny * nx
 
-    ring = Ring(nz, kbuf, vbuf, ring_recv, ring_send, pass_send)
+    ring = Ring(nz, kbuf, vbuf, *ring_sems)
     soft = Softmax(rows, tile, qz, kbuf, vbuf, top, acc, scores)
     projections = []
-    for axis, weight in zip(AXES, (wo_hbm, wd_hbm, sd_hbm)):
+    for axis, weight in zip(AXES, (wo_hbm, wo_hbm, wd_hbm, sd_hbm)):
         wb, hx, pr, rr, sems = take(5)
         projections.append(Projection(grid, axis, weight, wb, hx, pr, rr, sems))
-    out_proj, down, shared_down = projections
+    out_upper, out_lower, down, shared_down = projections
+    half = rows // 2
     routing = Routing(tokens, experts, cap)
 
     barrier = pltpu.get_barrier_semaphore()
@@ -608,10 +625,8 @@
     spread = Spread(grid, xg, g_sems)
     back = Exchange("ep", eps, lambda i: back_out.at[i], lambda i: back_in.at[i], back_in.at[slots], b_sems)
     there.start()
-    ring.start_own()
     down.start_weights()
     shared_down.start_weights()
-    out_proj.start_weights()
 
     q_load.wait()
     q = rotated(q_ref[...], cosine_ref[...], sine_ref[...]).astype(bf16).astype(f32) * 0.125
@@ -622,6 +637,8 @@
     weights[1].wait()
     with jax.named_scope("shared_diagonal"):
         shared_down.start_gather(swiglu(xn[...], sgu[...]))
+    ring.start_own()
+    with jax.named_scope("diagonal"):
         soft.diagonal(ep)
 
     @pl.when(ring.c == 1)
@@ -642,41 +659,43 @@
                 use(source)
 
     def use_down(t):
-        source, here = ring.down_source(t)
-
-        @pl.when(jnp.logical_and(jnp.logical_and(here, t >= 1), source < ring.z))
+        source, used = ring.down_used(t)
+
+        @pl.when(used)
         def _():
             with jax.named_scope("use_down"):
                 use(source)
 
+    with jax.named_scope("there_wait"):
+        there.wait()
+    rows_in = in_slots[...].reshape(experts * PAD, LANES)
+    rows_in = jnp.dot(routing.packing(False), rows_in, preferred_element_type=f32)
+    xg[:, block(tp)] = rows_in.astype(bf16)
+    spread.start()
+
     @pl.loop(1, ring.up_steps + 1)
     def _(t):
-        with jax.named_scope("serve_keys"):
+        with jax.named_scope("serve_0"):
             ring.serve(t, 0)
         use_up(t - 1)
-        with jax.named_scope("serve_values"):
+        with jax.named_scope("serve_1_2"):
             ring.serve(t, 1)
+            ring.serve(t, 2)
         use_down(t - 1)
-
-        @pl.when(t == SPREAD_AT)
-        def _():
-            with jax.named_scope("there_wait"):
-                there.wait()
-            rows_in = in_slots[...].reshape(experts * PAD, LANES)
-            rows_in = jnp.dot(routing.packing(False), rows_in, preferred_element_type=f32)
-            xg[:, block(tp)] = rows_in.astype(bf16)
-            spread.start()
+        with jax.named_scope("serve_3"):
+            ring.serve(t, 3)
+            ring.hand(t)
+
+        @pl.when(t == RELAY_AT)
+        def _():
+            with jax.named_scope("relay"):
+                spread.relay()
 
         @pl.when(t == SHARED_AT)
         def _():
             with jax.named_scope("shared_multiply"):
                 shared_down.wait_weights()
                 shared_down.multiply_and_send()
-
-        @pl.when(t == RELAY_AT)
-        def _():
-            with jax.named_scope("relay"):
-                spread.relay()
 
         @pl.when(t == EXPERT_AT)
         def _():
@@ -686,6 +705,8 @@
                 spread.wait()
             with jax.named_scope("experts"):
                 down.start_gather(swiglu(xg[...], wgu[...]))
+            out_upper.start_weights()
+            out_lower.start_weights()
 
         @pl.when(t == DOWN_AT)
         def _():
@@ -697,21 +718,24 @@
         def _():
             with jax.named_scope("down_finish"):
                 y = down.finish().astype(bf16)
-            y = jnp.dot(routing.packing(True), y, preferred_element_type=f32).astype(bf16)
-            back_out[...] = y.reshape(experts, PAD, LANES)
-            back_in[ep] = back_out[ep]
-            back.start()
+                y = jnp.dot(routing.packing(True), y, preferred_element_type=f32).astype(bf16)
+                back_out[...] = y.reshape(experts, PAD, LANES)
+                back_in[ep] = back_out[ep]
+                back.start()
 
     use_up(ring.up_steps)
     gain_load.wait()
     with jax.named_scope("heads"):
-        out_proj.start_gather(soft.heads(lam_ref[0], gain_ref[...]))
+        heads = soft.heads(lam_ref[0], gain_ref[...])
+        out_upper.start_gather(heads[:half])
+        out_lower.start_gather(heads[half:])
     with jax.named_scope("shared_finish"):
         mixed = shared_down.finish()
         chosen = routing.from_slots(routes_ref[...])
     with jax.named_scope("out_multiply"):
-        out_proj.wait_weights()
-        out_proj.multiply_and_send()
+        for projection in (out_upper, out_lower):
+            projection.wait_weights()
+            projection.multiply_and_send()
     rweight_load.wait()
     with jax.named_scope("back_wait"):
         back.wait()
@@ -723,7 +747,8 @@
     moe_store = pltpu.make_async_copy(moe_ref, moe_hbm, load_sem.at[0])
     moe_store.start()
     with jax.named_scope("out_finish"):
-        attn_ref[...] = out_proj.finish().astype(bf16)
+        attn_ref[:half, :] = out_upper.finish().astype(bf16)
+        attn_ref[half:, :] = out_lower.finish().astype(bf16)
     attn_store = pltpu.make_async_copy(attn_ref, attn_hbm, load_sem.at[1])
     attn_store.start()
     with jax.named_scope("wait_sends"):
@@ -774,9 +799,11 @@
         pltpu.VMEM((2 * rows, LANES), f32),
         pltpu.VMEM((2 * rows, 2 * LANES), f32),
         pltpu.VMEM((2, tile, CORES * rows), f32),
-        dma((slots, 2)),
-        dma((nz + 1, 2)),
-        dma((nz, 2)),
+        dma((nz, PARTS)),
+        dma((nz,)),
+        dma((PARTS,)),
+        dma((PARTS,)),
+        dma((2,)),
         pltpu.VMEM((tokens, width), bf16),
         pltpu.VMEM((width, 2 * LANES), bf16),
         pltpu.VMEM((width, 2 * LANES), bf16),
@@ -794,7 +821,7 @@
         pltpu.VMEM((rows, LANES), f32),
         pltpu.VMEM((rows, LANES), f32),
     ]
-    for axis, height in zip(AXES, (rows, experts * cap, tokens)):
+    for axis, height in zip(AXES, (rows // 2, rows // 2, experts * cap, tokens)):
         scratch += Projection.scratch(grid, axis, height)
     return tuple(
         pl.pallas_call(

time: 78.6 us -> 75.6 us (0.962)
  the two profiles are of different devices: /device:TPU:256 before, /device:TPU:1 now
where the time goes in v4:
time: 75.6 us; the launch traced here: 74.7 us
  Pallas kernels  71.2 us (94%)
  local copies, waits for them, and re-layouts  2.17 us (3%)
  between operations  1.3 us (2%)
    pallas_call x1, Pallas kernels, local(): pl.pallas_call(functools.partial(kernel, (nz, ny, nx, rows, tile, tokens,...  71.2 us
    unnamed x4, local copies, waits for them, and re-layouts  2.17 us

profile of v4, /device:TPU:1, one launch (start us, length us, event | category | flops | bytes accessed | tf_op | source)
XLA Modules:
  0.0 74.7 jit_solution(15880723159783347477)
XLA Ops:
  1.3 71.2 %layer.1 = (bf16[384,128]{1,0:T(8,128)(2,1)}, bf16[160,128]{1,0:T(8,128)(2,1)}) custom-call(bf16[384,128]{1,0:T(8,128)(2,1)} %refs_0_.1, bf16[384,128]{1,0:T(8,128)(2,1)} %refs_1_.1, f32[1,128]{1,0:T(1,128)} %constant.2.clone.refs_2_, f32[1,128]{1,0:T(1,128)} %bitcast.13, bf16[160,2048]{1,0:T(8,128)(2,1)} %refs_4_.1, f32[1,2048]{1,0:T(1,128)} %bitcast.10, ...), custom_call_target="tpu_custom_call" | custom-call | tf_op jit(solution)/shard_map/layer/pallas_call | solution.py:827
  72.5 0.0 copy-start
  72.5 1.5 %copy.22 = bf16[384,128]{1,0:T(8,128)(2,1)} copy(bf16[384,128]{1,0:T(8,128)(2,1)} %get-tuple-element.4) | data formatting | bytes 196608
  74.0 0.0 copy-done
  74.0 0.6 copy.23
Async XLA Ops:
  72.5 1.6 %copy-start = (bf16[160,128]{1,0:T(8,128)(2,1)S(1)}, bf16[160,128]{1,0:T(8,128)(2,1)}, u32[]{:S(2)}) copy-start(bf16[160,128]{1,0:T(8,128)(2,1)} %get-tuple-element.5) | copy-start | bytes 122884

commit v5 on v4

--- a/solution.py
+++ b/solution.py
@@ -23,7 +23,7 @@
 bf16 = jnp.bfloat16
 
 AXES = ("x", "y", "x", "y")
-RELAY_AT, SHARED_AT, EXPERT_AT, DOWN_AT, BACK_AT = 1, 3, 4, 6, 8
+RELAY_AT, SHARED_AT, EXPERT_AT, DOWN_AT, BACK_AT = 1, 3, 4, 6, 7
 
 
 def frequencies():
@@ -589,21 +589,13 @@
         sem = load_sem.at[len(loads) + i]
         weights.append(pltpu.make_async_copy(source, buf.at[:, pl.ds(k * LANES, LANES)], sem))
     v_load = pltpu.make_async_copy(v_hbm, vbuf.at[ep], load_sem.at[len(loads) + 4])
-    for load in (freq_load, k_load, v_load, x_load, fgain_load, routes_load, q_load, gain_load, rweight_load):
+    for load in (x_load, fgain_load, routes_load, freq_load, k_load, v_load, q_load, gain_load, rweight_load):
         load.start()
     for load in weights:
         load.start()
     for projection in projections:
         projection.start_own_weights()
 
-    with jax.named_scope("pre_angles"):
-        freq_load.wait()
-        cosine, sine = angle_tables(ep, rows, freq_ref[...])
-        cosine_ref[...] = cosine
-        sine_ref[...] = sine
-    with jax.named_scope("pre_keys"):
-        k_load.wait()
-        kbuf[ep] = jnp.transpose(rotated(k_ref[...], cosine_ref[...], sine_ref[...])).astype(bf16)
     with jax.named_scope("pre_norm"):
         x_load.wait()
         fgain_load.wait()
@@ -616,7 +608,6 @@
         sent = jnp.dot(to_slots, xn[:, block(tp)], preferred_element_type=f32).astype(bf16)
         out_slots[...] = sent.reshape(experts, PAD, LANES)
         in_slots[ep] = out_slots[ep]
-        v_load.wait()
 
     with jax.named_scope("barrier"):
         pl.semaphore_wait(barrier, eps + tps - 2)
@@ -628,6 +619,17 @@
     down.start_weights()
     shared_down.start_weights()
 
+    with jax.named_scope("pre_angles"):
+        freq_load.wait()
+        cosine, sine = angle_tables(ep, rows, freq_ref[...])
+        cosine_ref[...] = cosine
+        sine_ref[...] = sine
+    with jax.named_scope("pre_keys"):
+        k_load.wait()
+        kbuf[ep] = jnp.transpose(rotated(k_ref[...], cosine_ref[...], sine_ref[...])).astype(bf16)
+        v_load.wait()
+    ring.start_own()
+
     q_load.wait()
     q = rotated(q_ref[...], cosine_ref[...], sine_ref[...]).astype(bf16).astype(f32) * 0.125
     lane = lax.broadcasted_iota(jnp.int32, q.shape, 1)
@@ -637,7 +639,6 @@
     weights[1].wait()
     with jax.named_scope("shared_diagonal"):
         shared_down.start_gather(swiglu(xn[...], sgu[...]))
-    ring.start_own()
     with jax.named_scope("diagonal"):
         soft.diagonal(ep)
 
@@ -736,6 +737,13 @@
         for projection in (out_upper, out_lower):
             projection.wait_weights()
             projection.multiply_and_send()
+    with jax.named_scope("wait_sends"):
+        ring.wait_sends()
+    with jax.named_scope("out_finish"):
+        attn_ref[:half, :] = out_upper.finish().astype(bf16)
+        attn_ref[half:, :] = out_lower.finish().astype(bf16)
+    attn_store = pltpu.make_async_copy(attn_ref, attn_hbm, load_sem.at[1])
+    attn_store.start()
     rweight_load.wait()
     with jax.named_scope("back_wait"):
         back.wait()
@@ -746,15 +754,21 @@
     moe_ref[...] = mixed.astype(bf16)
     moe_store = pltpu.make_async_copy(moe_ref, moe_hbm, load_sem.at[0])
     moe_store.start()
-    with jax.named_scope("out_finish"):
-        attn_ref[:half, :] = out_upper.finish().astype(bf16)
-        attn_ref[half:, :] = out_lower.finish().astype(bf16)
-    attn_store = pltpu.make_async_copy(attn_ref, attn_hbm, load_sem.at[1])
-    attn_store.start()
-    with jax.named_scope("wait_sends"):
-        ring.wait_sends()
     moe_store.wait()
     attn_store.wait()
+
+
+def hand_over(*refs):
+    sources, targets, buffers, sems = refs[:2], refs[2:4], refs[4:6], refs[6]
+    loads = [pltpu.make_async_copy(a, b, sems.at[i]) for i, (a, b) in enumerate(zip(sources, buffers))]
+    stores = [pltpu.make_async_copy(a, b, sems.at[2 + i]) for i, (a, b) in enumerate(zip(buffers, targets))]
+    for load in loads:
+        load.start()
+    for load, store in zip(loads, stores):
+        load.wait()
+        store.start()
+    for store in stores:
+        store.wait()
 
 
 def local(
@@ -823,7 +837,7 @@
     ]
     for axis, height in zip(AXES, (rows // 2, rows // 2, experts * cap, tokens)):
         scratch += Projection.scratch(grid, axis, height)
-    return tuple(
+    results = (
         pl.pallas_call(
             functools.partial(kernel, (nz, ny, nx, rows, tile, tokens, experts, cap)),
             out_shape=[
@@ -857,6 +871,17 @@
             shared_down,
         )
     )
+    shapes = [jax.ShapeDtypeStruct(x.shape, x.dtype) for x in results]
+    return tuple(
+        pl.pallas_call(
+            hand_over,
+            out_shape=shapes,
+            in_specs=[hbm, hbm],
+            out_specs=[hbm, hbm],
+            scratch_shapes=[pltpu.VMEM(s.shape, s.dtype) for s in shapes] + [dma((4,))],
+            name="hand_over",
+        )(*results)
+    )
 
 
 def grid_of(mesh):

time: 75.6 us -> 72.4 us (0.958)
  local copies, waits for them, and re-layouts: 2.17 us -> 0 us
    unnamed x4 -> x0, local copies, waits for them, and re-layouts: 2.17 us -> none
    pallas_call x1, Pallas kernels: 71.2 us -> 69.3 us  [local(): pl.pallas_call(functools.partial(kernel, (nz, ny, nx, rows, tile, tokens,...]
    pallas_call x0 -> x1, Pallas kernels: none -> 1.58 us  [local(): pl.pallas_call(hand_over, out_shape=shapes, in_specs=[hbm, hbm], out_spec...]
where the time goes in v5:
time: 72.4 us; the launch traced here: 72.2 us
  Pallas kernels  70.9 us (98%)
  between operations  1.29 us (2%)
    pallas_call x1, Pallas kernels, local(): pl.pallas_call(functools.partial(kernel, (nz, ny, nx, rows, tile, tokens,...  69.3 us
    pallas_call x1, Pallas kernels, local(): pl.pallas_call(hand_over, out_shape=shapes, in_specs=[hbm, hbm], out_spec...  1.58 us

profile of v5, /device:TPU:1, one launch (start us, length us, event | category | flops | bytes accessed | tf_op | source)
XLA Modules:
  0.0 72.2 jit_solution(613553572161042673)
XLA Ops:
  1.3 69.3 %layer.1 = (bf16[384,128]{1,0:T(8,128)(2,1)}, bf16[160,128]{1,0:T(8,128)(2,1)}) custom-call(bf16[384,128]{1,0:T(8,128)(2,1)} %refs_0_.1, bf16[384,128]{1,0:T(8,128)(2,1)} %refs_1_.1, f32[1,128]{1,0:T(1,128)} %constant.2.clone.refs_2_, f32[1,128]{1,0:T(1,128)} %bitcast.13, bf16[160,2048]{1,0:T(8,128)(2,1)} %refs_4_.1, f32[1,2048]{1,0:T(1,128)} %bitcast.10, ...), custom_call_target="tpu_custom_call" | custom-call | tf_op jit(solution)/shard_map/layer/pallas_call | solution.py:841
  70.6 1.6 %hand_over.1 = (bf16[384,128]{1,0:T(8,128)(2,1)}, bf16[160,128]{1,0:T(8,128)(2,1)}) custom-call(bf16[384,128]{1,0:T(8,128)(2,1)} %get-tuple-element.4.refs_0_, bf16[160,128]{1,0:T(8,128)(2,1)} %get-tuple-element.5.refs_1_), custom_call_target="tpu_custom_call" | custom-call | tf_op jit(solution)/shard_map/hand_over/pallas_call | solution.py:876

commit v6 on v5

--- a/solution.py
+++ b/solution.py
@@ -23,6 +23,7 @@
 bf16 = jnp.bfloat16
 
 AXES = ("x", "y", "x", "y")
+SAME = (True, True, False, True)
 RELAY_AT, SHARED_AT, EXPERT_AT, DOWN_AT, BACK_AT = 1, 3, 4, 6, 7
 
 
@@ -73,11 +74,11 @@
 
 
 class Projection:
-    def __init__(self, grid, axis, w_hbm, wb, hx, pr, rr, sems):
+    def __init__(self, grid, axis, same, w_hbm, wb, hx, pr, rr, sems):
         self.ny, self.nx = grid
-        self.axis = axis
+        self.axis, self.same = axis, same
         self.w, self.wb, self.hx, self.pr, self.rr = w_hbm, wb, hx, pr, rr
-        names = ("w_send", "w_recv", "w_local", "h_send", "h_recv", "p_send", "p_recv")
+        names = ("w_send", "w_recv", "w_local", "h_send", "h_recv", "p_send", "p_recv", "d_send", "d_recv")
         for i, name in enumerate(names):
             setattr(self, name, sems.at[i])
         y, x = split_tp(self.nx)
@@ -93,29 +94,38 @@
             pltpu.VMEM((rows, ng * LANES), bf16),
             pltpu.VMEM((no, rows, LANES), bf16),
             pltpu.VMEM((no, rows, LANES), bf16),
-            dma((7,)),
+            dma((9,)),
         ]
 
     def _tp(self, g, o):
         return g * self.nx + o if self.axis == "y" else o * self.nx + g
 
-    def _weights(self, g):
-        rows = block(self.g)
+    def _weights(self, g, first, count):
+        source = pl.ds(first, count)
+        rows = pl.ds(pl.multiple_of(self.g * LANES + first, LANES // CORES), count)
         if self.axis == "y":
-            width = self.no * LANES
-            yield self.w.at[:, block(g, width)], self.wb.at[rows, :]
+            yield self.w.at[source, block(g, self.no * LANES)], self.wb.at[rows, :]
             return
         for o in range(self.no):
-            yield self.w.at[:, block(self._tp(g, o))], self.wb.at[rows, pl.ds(o * LANES, LANES)]
+            yield self.w.at[source, block(self._tp(g, o))], self.wb.at[rows, pl.ds(o * LANES, LANES)]
 
     def start_own_weights(self):
-        for source, target in self._weights(self.g):
+        for source, target in self._weights(self.g, 0, LANES):
             pltpu.make_async_copy(source, target, self.w_local).start()
+
+    def _share(self):
+        if not self.same:
+            return 0, LANES
+        count = LANES // CORES
+        return pl.multiple_of(lax.rem(self.ep, CORES) * count, count), count
+
+    def _others(self):
+        return self.wb.at[pl.ds(0, (self.ng - 1) * self._share()[1]), :]
 
     def start_weights(self):
         for i in range(1, self.ng):
             g = lax.rem(self.g + i, self.ng)
-            for source, target in self._weights(g):
+            for source, target in self._weights(g, *self._share()):
                 pltpu.make_async_remote_copy(
                     src_ref=source,
                     dst_ref=target,
@@ -125,11 +135,29 @@
                     device_id_type=MESH,
                 ).start()
 
+    def take_weights(self):
+        arrived(self._others(), self.w_recv)
+        arrived(self._others(), self.w_send)
+        if not self.same:
+            return
+        first, count = self._share()
+        for i in range(1, self.ng):
+            g = lax.rem(self.g + i, self.ng)
+            ref = self.wb.at[pl.ds(pl.multiple_of(g * LANES + first, count), count), :]
+            pltpu.make_async_remote_copy(
+                src_ref=ref,
+                dst_ref=ref,
+                send_sem=self.d_send,
+                recv_sem=self.d_recv,
+                device_id=(self.ep + 1 - 2 * lax.rem(self.ep, CORES), self._tp(self.g, self.o)),
+                device_id_type=MESH,
+            ).start()
+
     def wait_weights(self):
-        one, others = self.wb.at[pl.ds(0, LANES), :], self.wb.at[pl.ds(0, (self.ng - 1) * LANES), :]
-        arrived(one, self.w_local)
-        arrived(others, self.w_recv)
-        arrived(others, self.w_send)
+        arrived(self.wb.at[pl.ds(0, LANES), :], self.w_local)
+        if self.same:
+            arrived(self._others(), self.d_recv)
+            arrived(self._others(), self.d_send)
 
     def _gather(self, i):
         own = self.hx.at[:, block(self.g)]
@@ -566,9 +594,9 @@
     ring = Ring(nz, kbuf, vbuf, *ring_sems)
     soft = Softmax(rows, tile, qz, kbuf, vbuf, top, acc, scores)
     projections = []
-    for axis, weight in zip(AXES, (wo_hbm, wo_hbm, wd_hbm, sd_hbm)):
+    for axis, same, weight in zip(AXES, SAME, (wo_hbm, wo_hbm, wd_hbm, sd_hbm)):
         wb, hx, pr, rr, sems = take(5)
-        projections.append(Projection(grid, axis, weight, wb, hx, pr, rr, sems))
+        projections.append(Projection(grid, axis, same, weight, wb, hx, pr, rr, sems))
     out_upper, out_lower, down, shared_down = projections
     half = rows // 2
     routing = Routing(tokens, experts, cap)
@@ -618,6 +646,7 @@
     there.start()
     down.start_weights()
     shared_down.start_weights()
+    out_lower.start_weights()
 
     with jax.named_scope("pre_angles"):
         freq_load.wait()
@@ -691,12 +720,14 @@
         def _():
             with jax.named_scope("relay"):
                 spread.relay()
+            shared_down.take_weights()
 
         @pl.when(t == SHARED_AT)
         def _():
             with jax.named_scope("shared_multiply"):
                 shared_down.wait_weights()
                 shared_down.multiply_and_send()
+            out_lower.take_weights()
 
         @pl.when(t == EXPERT_AT)
         def _():
@@ -707,11 +738,11 @@
             with jax.named_scope("experts"):
                 down.start_gather(swiglu(xg[...], wgu[...]))
             out_upper.start_weights()
-            out_lower.start_weights()
 
         @pl.when(t == DOWN_AT)
         def _():
             with jax.named_scope("down_multiply"):
+                down.take_weights()
                 down.wait_weights()
                 down.multiply_and_send()
 
@@ -723,6 +754,7 @@
                 back_out[...] = y.reshape(experts, PAD, LANES)
                 back_in[ep] = back_out[ep]
                 back.start()
+            out_upper.take_weights()
 
     use_up(ring.up_steps)
     gain_load.wait()

time: 72.4 us -> 72.6 us (level)
  no operation moved by 1% of the time
where the time goes in v6:
time: 72.6 us; the launch traced here: 72.4 us
  Pallas kernels  71.1 us (98%)
  between operations  1.29 us (2%)
    pallas_call x1, Pallas kernels, local(): pl.pallas_call(functools.partial(kernel, (nz, ny, nx, rows, tile, tokens,...  69.5 us
    pallas_call x1, Pallas kernels, local(): pl.pallas_call(hand_over, out_shape=shapes, in_specs=[hbm, hbm], out_spec...  1.58 us

profile of v6, /device:TPU:1, one launch (start us, length us, event | category | flops | bytes accessed | tf_op | source)
XLA Modules:
  0.0 72.4 jit_solution(7321408818462349653)
XLA Ops:
  1.3 69.5 %layer.1 = (bf16[384,128]{1,0:T(8,128)(2,1)}, bf16[160,128]{1,0:T(8,128)(2,1)}) custom-call(bf16[384,128]{1,0:T(8,128)(2,1)} %refs_0_.1, bf16[384,128]{1,0:T(8,128)(2,1)} %refs_1_.1, f32[1,128]{1,0:T(1,128)} %constant.2.clone.refs_2_, f32[1,128]{1,0:T(1,128)} %bitcast.13, bf16[160,2048]{1,0:T(8,128)(2,1)} %refs_4_.1, f32[1,2048]{1,0:T(1,128)} %bitcast.10, ...), custom_call_target="tpu_custom_call" | custom-call | tf_op jit(solution)/shard_map/layer/pallas_call | solution.py:873
  70.8 1.6 %hand_over.1 = (bf16[384,128]{1,0:T(8,128)(2,1)}, bf16[160,128]{1,0:T(8,128)(2,1)}) custom-call(bf16[384,128]{1,0:T(8,128)(2,1)} %get-tuple-element.4.refs_0_, bf16[160,128]{1,0:T(8,128)(2,1)} %get-tuple-element.5.refs_1_), custom_call_target="tpu_custom_call" | custom-call | tf_op jit(solution)/shard_map/hand_over/pallas_call | solution.py:908
